TPU v7x, 256 devices: a 8x8x2 block of a 8x8x16 slice. The times are simulated.
256 devices in a mesh: grp: 2 (over z), ep: 64 (over y, x), tp: 2 (over core).
Axes of the slice: x: 8, y: 8, z: 2, core: 2. Of those that a mesh axis runs over, the one named last changes fastest.
The devices are a block of a 8x8x16 slice.
Arguments:
- tokens: bfloat16 [65536, 2048], P(('grp', 'ep', 'tp')), parts along dimension 0, may hold values from -6 to 6
- norm_gain: float32 [2048], replicated, may hold values from 0.1 to 1.9
- expert_ids: int32 [65536, 2], P(('grp', 'ep', 'tp')), parts along dimension 0, may hold values from 0 to 127, all different within a row; in each aligned block of 256 rows (0 to 255, 256 to 511, ...) at most 8 rows name the same one
- gate_values: float32 [65536, 2], P(('grp', 'ep', 'tp')), parts along dimension 0, may hold values from 0.2 to 2
- w_gate: bfloat16 [128, 2048, 512], P('ep', None, 'tp'), may hold values from -0.125 to 0.125
- w_up: bfloat16 [128, 2048, 512], P('ep', None, 'tp'), may hold values from -0.125 to 0.125
- w_down: bfloat16 [128, 512, 2048], P('ep', 'tp'), may hold values from -0.25 to 0.25
- s_gate: bfloat16 [2048, 512], P(None, 'tp'), may hold values from -0.125 to 0.125
- s_up: bfloat16 [2048, 512], P(None, 'tp'), may hold values from -0.125 to 0.125
- s_down: bfloat16 [512, 2048], P('tp'), may hold values from -0.25 to 0.25
Outputs:
- mixed: bfloat16 [65536, 2048], P(('grp', 'ep', 'tp')), parts along dimension 0
There are 2 independent parts, one for each index of `grp`. A program takes and returns all parts, laid end to end along the dimension named above; an argument that names none is the same for every part. Nothing has to cross between parts.
Inputs may be any that keep to these rules, and one draw needn't show every extreme that they name: `expert_ids`: each row names 2 different experts. Within the rows of one device no expert is named by more than 8 rows, a bound that some block reaches.
All inputs are finite; a program needn't handle non-finite values.
Results may differ from a plain program's by a relative error of at most 0.0068.
Values may be sent and summed in bfloat16 or wider, within the bound.
A program may use at most 128 MiB of HBM per device.

v0:
```python
import jax
import jax.numpy as jnp
from jax import lax
from jax.sharding import PartitionSpec as P


def in_one_piece(arrays, axis, dim, along):
    ends, at = ([], 0)
    for a in arrays[:-1]:
        at += a.shape[along]
        ends.append(at)
    both = jnp.concatenate(arrays, axis=along)
    return tuple(jnp.split(lax.all_gather(both, axis, axis=dim, tiled=True), ends, axis=along))


def cut_along(array, dim, devices):
    before, after = (array.shape[:dim], array.shape[dim + 1 :])
    return jnp.moveaxis(array.reshape(*before, devices, -1, *after), dim, 0)


def piece_ends(length, count):
    lap = length // count
    if lap >= 8:
        lap -= lap % 8
    return [lap * k for k in range(1, count)]


def laid_out(blocks, dim):
    shape = list(blocks.shape[1:])
    shape[dim] *= blocks.shape[0]
    return jnp.moveaxis(blocks, 0, dim).reshape(shape)


def exchange_in_pieces(array, axis, pieces, split_dim, concat_dim):
    blocks = cut_along(array, split_dim, lax.axis_size(axis))
    cut = max(range(1, max(2, blocks.ndim - 1)), key=lambda d: blocks.shape[d])
    done = []
    for section in jnp.split(blocks, piece_ends(blocks.shape[cut], pieces), axis=cut):
        if section.size:
            done.append(lax.all_to_all(section, axis, split_axis=0, concat_axis=0, tiled=True))
    return laid_out(jnp.concatenate(done, axis=cut), concat_dim)


def swiglu_rows(rows, first_w, second_w):
    first = jnp.einsum("xecd,edf->xecf", rows, first_w, preferred_element_type=jnp.float32)
    second = jnp.einsum("xecd,edf->xecf", rows, second_w, preferred_element_type=jnp.float32)
    return (jax.nn.silu(first) * second).astype(jnp.bfloat16)


def shared_swiglu(rows, first_w, second_w):
    first = jnp.dot(rows, first_w, preferred_element_type=jnp.float32)
    second = jnp.dot(rows, second_w, preferred_element_type=jnp.float32)
    return (jax.nn.silu(first) * second).astype(jnp.bfloat16)


def body(tokens, norm_gain, expert_ids, gate_values, w_gate, w_up, w_down, s_gate, s_up, s_down):
    n_rows, width = tokens.shape
    topk = expert_ids.shape[1]
    ep_size = lax.axis_size("ep")
    local_exp = w_gate.shape[0]
    experts_n = local_exp * ep_size
    capacity = 2 * n_rows * topk // experts_n
    xf = tokens.astype(jnp.float32)
    scale = lax.rsqrt(jnp.mean(xf * xf, axis=-1, keepdims=True) + 1e-06)
    normed = (xf * scale * norm_gain).astype(jnp.bfloat16)
    whole_sgate, whole_sup = in_one_piece((s_gate, s_up), "tp", 1, 0)
    whole_sdown = lax.all_gather(s_down, "tp", axis=0, tiled=True)
    s_hidden = shared_swiglu(normed, whole_sgate, whole_sup)
    shared = jnp.dot(s_hidden, whole_sdown, preferred_element_type=jnp.float32)
    flat_e = expert_ids.reshape(-1)
    onehot = (flat_e[:, None] == jnp.arange(experts_n, dtype=jnp.int32)[None, :]).astype(jnp.int32)
    before = jnp.cumsum(onehot, axis=0) - onehot
    slot = jnp.sum(before * onehot, axis=1)
    position = flat_e * capacity + slot
    flat_tok = jnp.arange(flat_e.shape[0], dtype=jnp.int32) // topk
    slot_tok = jnp.full((experts_n * capacity,), n_rows, jnp.int32).at[position].set(flat_tok)
    padded = jnp.concatenate([normed, jnp.zeros((1, width), jnp.bfloat16)], axis=0)
    outgoing = padded[slot_tok].reshape(ep_size, local_exp, capacity, width)
    arrived = lax.all_to_all(outgoing, "ep", split_axis=0, concat_axis=0, tiled=True)
    full_gate, full_up = (
        lax.all_gather(w_gate, "tp", axis=2, tiled=True),
        lax.all_gather(w_up, "tp", axis=2, tiled=True),
    )
    full_down = lax.all_gather(w_down, "tp", axis=1, tiled=True)
    hidden = swiglu_rows(arrived, full_gate, full_up)
    results = jnp.einsum("xecf,efd->xecd", hidden, full_down, preferred_element_type=jnp.float32)
    returned = exchange_in_pieces(results.astype(jnp.bfloat16), "ep", 2, 0, 0)
    picked = returned.reshape(experts_n * capacity, width)[position].reshape(n_rows, topk, width)
    routed = jnp.sum(gate_values[:, :, None] * picked.astype(jnp.float32), axis=1)
    return (shared + routed).astype(jnp.bfloat16)


def solution(mesh):
    return jax.shard_map(
        body,
        mesh=mesh,
        in_specs=(
            P(("grp", "ep", "tp"), None),
            P(),
            P(("grp", "ep", "tp"), None),
            P(("grp", "ep", "tp"), None),
            P("ep", None, "tp"),
            P("ep", None, "tp"),
            P("ep", "tp", None),
            P(None, "tp"),
            P(None, "tp"),
            P("tp", None),
        ),
        out_specs=P(("grp", "ep", "tp"), None),
        check_vma=False,
    )
```

profile of v0, /device:TPU:640, one launch (start us, length us, event | category | flops | bytes accessed | tf_op | source)
XLA Modules:
  0.0 344.6 jit_solution(617067628010789083)
XLA Ops:
  6.6 0.7 all-gather.10.cloned.1.call-update
  7.5 0.1 eq.29
  7.6 0.1 eq.25
  7.9 0.2 fusion.46
  8.3 0.1 mul.70
  8.5 0.3 fusion.11
  8.8 0.3 fusion.13
  9.3 0.2 fusion.45
  9.5 2.4 scatter_custom_fusion
  12.0 6.0 %gather_fusion = bf16[1024,2048]{1,0:T(8,128)(2,1)} fusion(bf16[257,2048]{1,0:T(8,128)(2,1)S(1)} %concatenate.10, s32[1024]{0:T(1024)S(1)} %fusion.50), kind=kCustom, calls=%fused_computation | custom fusion | bytes 8392704 | tf_op jit(solution)/shard_map/gather | solution.py:78
  18.0 21.3 %all-to-all-start = ((bf16[64,2,8,2048]{3,2,1,0:T(8,128)(2,1)}), bf16[64,2,8,2048]{3,2,1,0:T(8,128)(2,1)}, u32[]{:S(2)}, u32[]{:S(2)}) async-start(bf16[64,2,8,2048]{3,2,1,0:T(8,128)(2,1)} %bitcast.69), calls=%async_computation | async-start | bytes 8388608 | tf_op jit(solution)/shard_map/all_to_all | solution.py:79
  39.4 0.7 all-gather.12.cloned.1.call-update
  40.1 0.2 all-gather.14.cloned.1.call-start
  40.3 0.5 all-gather.14.cloned.1.call-update
  40.9 101.3 %all-to-all-done = bf16[64,2,8,2048]{3,2,1,0:T(8,128)(2,1)} async-done(((bf16[64,2,8,2048]{3,2,1,0:T(8,128)(2,1)}), bf16[64,2,8,2048]{3,2,1,0:T(8,128)(2,1)}, u32[]{:S(2)}, u32[]{:S(2)}) %all-to-all-start) | async-done | bytes 4194336 | tf_op jit(solution)/shard_map/all_to_all | solution.py:79
  142.2 5.8 %fusion.4 = f32[2,64,8,512]{3,2,1,0:T(8,128)S(1)} fusion(bf16[2,2048,512]{2,1,0:T(8,128)(2,1)} %all-gather.10.cloned.1.call-done, bf16[64,2,8,2048]{3,2,1,0:T(8,128)(2,1)} %all-to-all-done), kind=kOutput, calls=%fused_computation.8 | convolution fusion | flops 2147483648 | bytes 10485760 | tf_op jit(solution)/shard_map/xecd,edf->xecf/dot_general | solution.py:45
  148.1 11.2 %convert_bitcast_fusion = bf16[64,1,2,8,2048]{4,3,0,2,1:T(8,128)(2,1)} fusion(bf16[2,512,2048]{2,1,0:T(8,128)(2,1)} %all-gather.14.cloned.1.call-done, f32[2,64,8,512]{3,2,1,0:T(8,128)S(1)} %fusion.4, bf16[2,2048,512]{2,1,0:T(8,128)(2,1)} %all-gather.12.cloned.1.call-done, bf16[64,2,8,2048]{3,2,1,0:T(8,128)(2,1)} %all-to-all-done), kind=kOutput, calls=%fused_computation.11 | convolution fusion | flops 4300210176 | bytes 18874368 | tf_op jit(solution)/shard_map/xecf,efd->xecd/dot_general | solution.py:86
  159.2 6.6 %fusion.58 = (bf16[64,1,2,4,2048]{4,3,0,2,1:T(4,128)(2,1)S(1)}, bf16[64,1,2,4,2048]{4,3,0,2,1:T(4,128)(2,1)}) fusion(bf16[64,1,2,8,2048]{4,3,0,2,1:T(8,128)(2,1)} %convert_bitcast_fusion), kind=kLoop, calls=%fused_computation.69 | loop fusion | bytes 8388608 | tf_op jit(solution)/shard_map/split | solution.py:38
  165.8 2.7 copy.28
  168.6 31.1 %all-to-all-start.1 = ((bf16[64,1,2,4,2048]{4,3,2,1,0:T(4,128)(2,1)}), bf16[64,1,2,4,2048]{4,3,2,1,0:T(4,128)(2,1)S(1)}, u32[]{:S(2)}, u32[]{:S(2)}) async-start(bf16[64,1,2,4,2048]{4,3,2,1,0:T(4,128)(2,1)} %copy.28), calls=%async_computation.1 | async-start | bytes 4194304 | tf_op jit(solution)/shard_map/all_to_all | solution.py:40
  199.8 3.0 pad_maximum_fusion.1
  202.9 4.3 %copy.29 = bf16[64,1,2,4,2048]{4,3,2,1,0:T(4,128)(2,1)} copy(bf16[64,1,2,4,2048]{4,3,0,2,1:T(4,128)(2,1)} %get-tuple-element.6) | data formatting | bytes 4194304 | tf_op jit(solution)/shard_map/split | solution.py:38
  207.2 43.2 %all-to-all-done.1 = bf16[64,1,2,4,2048]{4,3,2,1,0:T(4,128)(2,1)S(1)} async-done(((bf16[64,1,2,4,2048]{4,3,2,1,0:T(4,128)(2,1)}), bf16[64,1,2,4,2048]{4,3,2,1,0:T(4,128)(2,1)S(1)}, u32[]{:S(2)}, u32[]{:S(2)}) %all-to-all-start.1) | async-done | bytes 2097184 | tf_op jit(solution)/shard_map/all_to_all | solution.py:40
  250.4 9.0 %all-to-all-start.2 = ((bf16[64,1,2,4,2048]{4,3,2,1,0:T(4,128)(2,1)}), bf16[64,1,2,4,2048]{4,3,2,1,0:T(4,128)(2,1)}, u32[]{:S(2)}, u32[]{:S(2)}) async-start(bf16[64,1,2,4,2048]{4,3,2,1,0:T(4,128)(2,1)} %copy.29), calls=%async_computation.2 | async-start | bytes 4194304 | tf_op jit(solution)/shard_map/all_to_all | solution.py:40
  259.6 0.6 all-gather.8.cloned.1.call-update
  260.3 3.1 fusion.16
  263.4 45.2 %all-to-all-done.2 = bf16[64,1,2,4,2048]{4,3,2,1,0:T(4,128)(2,1)} async-done(((bf16[64,1,2,4,2048]{4,3,2,1,0:T(4,128)(2,1)}), bf16[64,1,2,4,2048]{4,3,2,1,0:T(4,128)(2,1)}, u32[]{:S(2)}, u32[]{:S(2)}) %all-to-all-start.2) | async-done | bytes 2097184 | tf_op jit(solution)/shard_map/all_to_all | solution.py:40
  308.6 4.7 %pad_maximum_fusion = bf16[64,1,2,8,2048]{4,3,2,0,1:T(8,128)(2,1)} fusion(bf16[64,1,2,4,2048]{4,3,2,0,1:T(4,128)(2,1)} %bitcast.18, bf16[64,1,2,4,2048]{4,3,2,0,1:T(4,128)(2,1)S(1)} %bitcast.70), kind=kLoop, calls=%fused_computation.3 | loop fusion | flops 8388608 | bytes 8388608 | tf_op jit(solution)/shard_map/concatenate | solution.py:41
  313.4 7.1 %gather_fusion.1 = bf16[512,2048]{1,0:T(8,128)(2,1)S(1)} fusion(bf16[1024,2048]{1,0:T(8,128)(2,1)} %bitcast.68, s32[1024]{0:T(1024)S(1)} %pad_clamp_fusion), kind=kCustom, calls=%fused_computation.1 | custom fusion | bytes 4196352 | tf_op jit(solution)/shard_map/gather | solution.py:88
  320.5 4.0 %reshape.68 = f32[256,2,2048]{2,1,0:T(2,128)} reshape(bf16[512,2048]{1,0:T(8,128)(2,1)S(1)} %gather_fusion.1) | data formatting | bytes 6291456 | tf_op jit(solution)/shard_map/convert_element_type | solution.py:89
  324.5 8.8 %multiply_reduce_fusion = f32[256,2048]{1,0:T(8,128)S(1)} fusion(f32[256,2,2048]{2,1,0:T(2,128)} %reshape.68, f32[256,2]{1,0:T(8,128)S(1)} %copy.20), kind=kLoop, calls=%fused_computation.10 | loop fusion | flops 1572864 | bytes 6293504 | tf_op jit(solution)/shard_map/reduce_sum | solution.py:89
  333.3 4.7 %fusion.10 = bf16[256,2048]{1,0:T(8,128)(2,1)} fusion(f32[256,2048]{1,0:T(8,128)S(1)} %multiply_reduce_fusion, bf16[512,2048]{1,0:T(8,128)(2,1)} %all-gather.8.cloned.1.call-done, bf16[256,2048]{1,0:T(8,128)(2,1)S(1)} %fusion.13, bf16[4096,512]{1,0:T(8,128)(2,1)} %all-gather.6.cloned.1.call-done, f32[256,512]{1,0:T(8,128)} %fusion.16), kind=kOutput, calls=%fused_computation.17 | convolution fusion | flops 1075576832 | bytes 8912896 | tf_op jit(solution)/shard_map/dot_general | solution.py:69
  (35 shorter events, 1.1 us)
Async XLA Ops:
  6.5 0.8 copy-start.2
  6.5 1.9 copy-start
  6.6 34.4 %all-gather.10.cloned.1.call-start = ((), (), s32[]{:S(2)}) async-start(), calls=%async_computation.5 | async-start | bytes 6291456 | tf_op jit(solution)/shard_map/all_gather | solution.py:81
  7.3 1.5 copy-start.1
  18.0 124.3 %all-to-all-start = ((bf16[64,2,8,2048]{3,2,1,0:T(8,128)(2,1)}), bf16[64,2,8,2048]{3,2,1,0:T(8,128)(2,1)}, u32[]{:S(2)}, u32[]{:S(2)}) async-start(bf16[64,2,8,2048]{3,2,1,0:T(8,128)(2,1)} %bitcast.69), calls=%async_computation | async-start | bytes 8388608 | tf_op jit(solution)/shard_map/all_to_all | solution.py:79
  39.3 108.8 %all-gather.12.cloned.1.call-start = ((), (), s32[]{:S(2)}) async-start(), calls=%async_computation.6 | async-start | bytes 6291456 | tf_op jit(solution)/shard_map/all_gather | solution.py:82
  40.1 108.0 %all-gather.14.cloned.1.call-start = ((), (), s32[]{:S(2)}) async-start(), calls=%async_computation.7 | async-start | bytes 6291456 | tf_op jit(solution)/shard_map/all_gather | solution.py:84
  168.6 81.9 %all-to-all-start.1 = ((bf16[64,1,2,4,2048]{4,3,2,1,0:T(4,128)(2,1)}), bf16[64,1,2,4,2048]{4,3,2,1,0:T(4,128)(2,1)S(1)}, u32[]{:S(2)}, u32[]{:S(2)}) async-start(bf16[64,1,2,4,2048]{4,3,2,1,0:T(4,128)(2,1)} %copy.28), calls=%async_computation.1 | async-start | bytes 4194304 | tf_op jit(solution)/shard_map/all_to_all | solution.py:40
  199.7 60.6 %all-gather.6.cloned.1.call-start = ((), (), s32[]{:S(2)}) async-start(), calls=%async_computation.3 | async-start | bytes 6291456 | tf_op jit(solution)/shard_map/all_gather | solution.py:13
  207.2 52.9 %copy-start.3 = (f32[256,2]{0,1:T(2,128)S(1)}, f32[256,2]{0,1:T(2,128)}, u32[]{:S(2)}) copy-start(f32[256,2]{0,1:T(2,128)} %param.13) | copy-start | bytes 6148
  250.4 58.2 %all-to-all-start.2 = ((bf16[64,1,2,4,2048]{4,3,2,1,0:T(4,128)(2,1)}), bf16[64,1,2,4,2048]{4,3,2,1,0:T(4,128)(2,1)}, u32[]{:S(2)}, u32[]{:S(2)}) async-start(bf16[64,1,2,4,2048]{4,3,2,1,0:T(4,128)(2,1)} %copy.29), calls=%async_computation.2 | async-start | bytes 4194304 | tf_op jit(solution)/shard_map/all_to_all | solution.py:40
  259.5 73.8 %all-gather.8.cloned.1.call-start = ((), (), s32[]{:S(2)}) async-start(), calls=%async_computation.4 | async-start | bytes 3145728 | tf_op jit(solution)/shard_map/all_gather | solution.py:67
Sparse Core Ops, SparseCore 0:
  9.2 27.7 all-gather.9
  41.9 20.1 all-gather.11
  63.9 21.8 all-gather.13
  203.0 20.1 all-gather.5
  261.8 17.9 all-gather.7
where the time goes:
time: 345 us
  waiting for transfers between devices  192 us (56%)
  starting transfers between devices  61.9 us (18%)
  local copies, waits for them, and re-layouts  34.3 us (10%)
  matrix products  24.8 us (7%)
  other arithmetic  17.7 us (5%)
  between operations  13.4 us (4%)
    all_to_all x1, waiting for transfers between devices, body(): lax.all_to_all(outgoing, 'ep', split_axis=0, concat_axis=0, tiled=True)  101 us
    all_to_all x2, waiting for transfers between devices, exchange_in_pieces(): lax.all_to_all(section, axis, split_axis=0, concat_axis=0, tiled=True)  88.4 us
    all_to_all x2, starting transfers between devices, exchange_in_pieces(): lax.all_to_all(section, axis, split_axis=0, concat_axis=0, tiled=True)  40.2 us
    all_to_all x1, starting transfers between devices, body(): lax.all_to_all(outgoing, 'ep', split_axis=0, concat_axis=0, tiled=True)  21.3 us
    split x3, local copies, waits for them, and re-layouts, exchange_in_pieces(): jnp.split(blocks, piece_ends(blocks.shape[cut], pieces), axis=cut)  13.7 us
    dot_general x1, matrix products, body(): jnp.einsum('xecf,efd->xecd', hidden, full_down, preferred_element_type=jn...  11.2 us
    reduce_sum x1, other arithmetic, body(): jnp.sum(gate_values[:, :, None] * picked.astype(jnp.float32), axis=1)  8.79 us
    gather x1, local copies, waits for them, and re-layouts, body(): returned.reshape(experts_n * capacity, width)[position]  7.13 us
  transfers between devices with their start and end apart: 8, of which 3 were waited for; matrix products, arithmetic and copies ran while one was open for 15% of the time, Pallas kernels for 0%

commit v1 on v0

v1 whole, which is shorter than its diff:
```python
import functools
import math

import jax
import jax.numpy as jnp
from jax import lax
from jax.experimental import pallas as pl
from jax.experimental.pallas import tpu as pltpu
from jax.sharding import PartitionSpec as P

MESH = pl.DeviceIdType.MESH
BF16, F32 = jnp.bfloat16, jnp.float32


def silu_mul(first, second):
    return first * (1.0 / (1.0 + jnp.exp(-first))) * second


def kernel(
    n_ep,
    topk,
    cap,
    tokens,
    gain,
    ids,
    ids_t,
    gates,
    w_gate,
    w_up,
    w_down,
    s_gate,
    s_up,
    s_down,
    out,
    normed,
    sent,
    arrived,
    results,
    returned,
    hidden,
    total,
    wg,
    wu,
    wd,
    sg,
    su,
    sd,
    local_sem,
    w_send,
    w_recv,
    go_send,
    go_recv,
    back_send,
    back_recv,
):
    n_rows, width = tokens.shape
    local_exp = w_gate.shape[0]
    half = w_gate.shape[2]
    experts = local_exp * n_ep
    side = math.isqrt(n_ep)
    slab = local_exp * cap
    chunk = side * slab
    me = lax.axis_index("ep")
    tp = lax.axis_index("tp")
    my_y, my_x = me // side, lax.rem(me, side)

    barrier = pltpu.get_barrier_semaphore()
    pl.semaphore_signal(barrier, inc=1, device_id={"tp": 1 - tp}, device_id_type=MESH)

    def greet(i, carry):
        peer = lax.rem(me + i, n_ep)
        pl.semaphore_signal(barrier, inc=1, device_id={"ep": peer}, device_id_type=MESH)
        return carry

    lax.fori_loop(1, n_ep, greet, 0)

    pairs = ((s_gate, sg), (s_up, su), (s_down, sd), (w_gate, wg), (w_up, wu), (w_down, wd))
    local = [
        pltpu.make_async_copy(src, dst.at[tp], local_sem.at[i])
        for i, (src, dst) in enumerate(pairs)
    ]
    remote = [
        pltpu.make_async_remote_copy(
            src_ref=src,
            dst_ref=dst.at[tp],
            send_sem=w_send.at[i],
            recv_sem=w_recv.at[i],
            device_id={"tp": 1 - tp},
            device_id_type=MESH,
        )
        for i, (src, dst) in enumerate(pairs)
    ]
    for copy in local:
        copy.start()

    step = min(32, n_rows)

    def norm(i, carry):
        rows = pl.ds(pl.multiple_of(i * step, step), step)
        xf = tokens[rows, :].astype(F32)
        scale = lax.rsqrt(jnp.mean(xf * xf, axis=-1, keepdims=True) + 1e-06)
        normed[rows, :] = (xf * scale * gain[...]).astype(BF16)
        return carry

    lax.fori_loop(0, n_rows // step, norm, 0)

    expert_of = lax.broadcasted_iota(jnp.int32, (n_rows, experts), 1)
    picks = [ids[:, k : k + 1] == expert_of for k in range(topk)]
    used = sum(p.astype(F32) for p in picks)
    earlier = (
        lax.broadcasted_iota(jnp.int32, (n_rows, n_rows), 1)
        < lax.broadcasted_iota(jnp.int32, (n_rows, n_rows), 0)
    ).astype(F32)
    place = jnp.dot(earlier.astype(BF16), used.astype(BF16), preferred_element_type=F32)
    place = place + (expert_of * cap).astype(F32)
    row_col = [
        jnp.sum(jnp.where(p, place, 0.0), axis=1, keepdims=True).astype(jnp.int32) for p in picks
    ]
    expert_of_t = lax.broadcasted_iota(jnp.int32, (experts, n_rows), 0)
    picks_t = [ids_t[k : k + 1, :] == expert_of_t for k in range(topk)]
    used_t = sum(p.astype(F32) for p in picks_t)
    earlier_t = (
        lax.broadcasted_iota(jnp.int32, (n_rows, n_rows), 0)
        < lax.broadcasted_iota(jnp.int32, (n_rows, n_rows), 1)
    ).astype(F32)
    place_t = jnp.dot(used_t.astype(BF16), earlier_t.astype(BF16), preferred_element_type=F32)
    place_t = place_t + (expert_of_t * cap).astype(F32)
    row_lane = [
        jnp.sum(jnp.where(p, place_t, 0.0), axis=0, keepdims=True).astype(jnp.int32)
        for p in picks_t
    ]

    pl.semaphore_wait(barrier, n_ep)
    for copy in remote:
        copy.start()

    def line_of(k, sign):
        return lax.rem(my_y + sign * k + side, side)

    def order(i):
        return lax.rem(jnp.where(lax.rem(i, 2) == 1, (i + 1) // 2, side - i // 2), side)

    def go(y, x, k):
        peer = y * side + x
        return pltpu.make_async_remote_copy(
            src_ref=sent.at[peer],
            dst_ref=arrived.at[me],
            send_sem=go_send.at[k],
            recv_sem=go_recv.at[k],
            device_id={"ep": peer},
            device_id_type=MESH,
        )

    def back(y, x, k):
        peer = y * side + x
        return pltpu.make_async_remote_copy(
            src_ref=results.at[peer],
            dst_ref=returned.at[me],
            send_sem=back_send.at[k],
            recv_sem=back_recv.at[k],
            device_id={"ep": peer},
            device_id_type=MESH,
        )

    def to_line(copy_of, y, k):
        def one(j, carry):
            copy_of(y, lax.rem(my_x + j, side), k).start()
            return carry

        @pl.when(k == 0)
        def _():
            lax.fori_loop(1, side, one, 0)

        @pl.when(k != 0)
        def _():
            lax.fori_loop(0, side, one, 0)

    def wait_line(buffer, sem, count):
        part = buffer.at[pl.ds(0, count)]
        pltpu.make_async_copy(part, part, sem).wait()

    def dispatch(i, carry):
        k = order(i)
        y = line_of(k, 1)
        row = lax.broadcasted_iota(jnp.int32, (chunk, n_rows), 0) + y * chunk
        pick = functools.reduce(jnp.logical_or, [row == lane for lane in row_lane])
        pick = pick.astype(F32).astype(BF16)
        for at in range(0, width, 512):
            part = jnp.dot(pick, normed[:, at : at + 512], preferred_element_type=F32)
            sent[pl.ds(pl.multiple_of(y * side, side), side), :, at : at + 512] = part.astype(
                BF16
            ).reshape(side, slab, 512)
        to_line(go, y, k)
        return carry

    lax.fori_loop(0, side, dispatch, 0)
    own = pltpu.make_async_copy(sent.at[me], arrived.at[me], go_recv.at[0])
    own.start()

    for copy in local:
        copy.wait()
    for copy in remote:
        copy.wait_recv()

    tile = min(256, n_rows)

    def shared(i, carry):
        rows = pl.ds(pl.multiple_of(i * tile, tile), tile)
        x = normed[rows, :]
        parts = []
        for h in range(2):
            first = jnp.dot(x, sg[h], preferred_element_type=F32)
            second = jnp.dot(x, su[h], preferred_element_type=F32)
            parts.append(silu_mul(first, second).astype(BF16))
        hid = jnp.concatenate(parts, axis=1)

        def down(n, carry):
            cols = pl.ds(pl.multiple_of(n * 256, 256), 256)
            w = sd[:, :, cols].reshape(2 * sd.shape[1], 256)
            total[rows, cols] = jnp.dot(hid, w, preferred_element_type=F32)
            return carry

        return lax.fori_loop(0, width // 256, down, carry)

    lax.fori_loop(0, n_rows // tile, shared, 0)

    expert_row = lax.rem(
        lax.broadcasted_iota(jnp.int32, (chunk, half), 0) // cap, local_exp
    )

    def experts_of(i, carry):
        k = order(i)
        y = line_of(k, -1)
        wait_line(arrived, go_recv.at[k], side)
        lines = pl.ds(pl.multiple_of(y * side, side), side)
        x = arrived[lines].reshape(chunk, width)

        def up(m, carry):
            h, j = m // local_exp, lax.rem(m, local_exp)
            first = jnp.dot(x, wg[h, j], preferred_element_type=F32)
            second = jnp.dot(x, wu[h, j], preferred_element_type=F32)
            both = jnp.where(expert_row == j, silu_mul(first, second), 0.0)
            hidden[:, pl.ds(pl.multiple_of(m * half, half), half)] = both.astype(BF16)
            return carry

        lax.fori_loop(0, 2 * local_exp, up, 0)

        def down(n, carry):
            cols = pl.ds(pl.multiple_of(n * 256, 256), 256)
            w = wd[:, :, :, cols].reshape(2 * local_exp * half, 256)
            part = jnp.dot(hidden[...], w, preferred_element_type=F32)
            results[lines, :, cols] = part.astype(BF16).reshape(side, slab, 256)
            return carry

        lax.fori_loop(0, width // 256, down, 0)
        to_line(back, y, k)
        return carry

    lax.fori_loop(0, side, experts_of, 0)
    pltpu.make_async_copy(results.at[me], returned.at[me], back_recv.at[0]).start()

    def combine(i, carry):
        k = order(i)
        y = line_of(k, 1)
        wait_line(returned, back_recv.at[k], side)
        row = lax.broadcasted_iota(jnp.int32, (n_rows, chunk), 1) + y * chunk
        weight = sum(
            jnp.where(row == row_col[j], gates[:, j : j + 1], 0.0) for j in range(topk)
        )
        high = weight.astype(BF16)
        low = (weight - high.astype(F32)).astype(BF16)
        lines = pl.ds(pl.multiple_of(y * side, side), side)

        def add(n, carry):
            cols = pl.ds(pl.multiple_of(n * 256, 256), 256)
            part = returned[lines, :, cols].reshape(chunk, 256)
            total[:, cols] += jnp.dot(high, part, preferred_element_type=F32) + jnp.dot(
                low, part, preferred_element_type=F32
            )
            return carry

        return lax.fori_loop(0, width // 256, add, carry)

    lax.fori_loop(0, side, combine, 0)

    def finish(i, carry):
        rows = pl.ds(pl.multiple_of(i * step, step), step)
        out[rows, :] = total[rows, :].astype(BF16)
        return carry

    lax.fori_loop(0, n_rows // step, finish, 0)

    for copy in remote:
        copy.wait_send()
    for k in range(side):
        count = side - 1 if k == 0 else side
        wait_line(sent, go_send.at[k], count)
        wait_line(results, back_send.at[k], count)


def body(n_ep, tokens, norm_gain, expert_ids, gate_values, w_gate, w_up, w_down, s_gate, s_up, s_down):
    n_rows, width = tokens.shape
    topk = expert_ids.shape[1]
    local_exp, _, half = w_gate.shape
    experts = local_exp * n_ep
    cap = 2 * n_rows * topk // experts
    side = math.isqrt(n_ep)
    slab = local_exp * cap
    chunk = side * slab
    vmem = pl.BlockSpec(memory_space=pltpu.VMEM)
    hbm = pl.BlockSpec(memory_space=pl.ANY)
    slabs = pltpu.VMEM((n_ep, slab, width), BF16)
    dma = pltpu.SemaphoreType.DMA
    return pl.pallas_call(
        functools.partial(kernel, n_ep, topk, cap),
        out_shape=jax.ShapeDtypeStruct((n_rows, width), BF16),
        in_specs=[vmem] * 5 + [hbm] * 6,
        out_specs=vmem,
        scratch_shapes=[
            pltpu.VMEM((n_rows, width), BF16),
            slabs,
            slabs,
            slabs,
            slabs,
            pltpu.VMEM((chunk, 2 * local_exp * half), BF16),
            pltpu.VMEM((n_rows, width), F32),
            pltpu.VMEM((2,) + w_gate.shape, BF16),
            pltpu.VMEM((2,) + w_up.shape, BF16),
            pltpu.VMEM((2,) + w_down.shape, BF16),
            pltpu.VMEM((2,) + s_gate.shape, BF16),
            pltpu.VMEM((2,) + s_up.shape, BF16),
            pltpu.VMEM((2,) + s_down.shape, BF16),
            dma((6,)),
            dma((6,)),
            dma((6,)),
            dma((side,)),
            dma((side,)),
            dma((side,)),
            dma((side,)),
        ],
        compiler_params=pltpu.CompilerParams(
            collective_id=0, has_side_effects=True, vmem_limit_bytes=58 * 1024 * 1024
        ),
    )(
        tokens,
        norm_gain.reshape(1, width),
        expert_ids,
        expert_ids.T,
        gate_values,
        w_gate,
        w_up,
        w_down,
        s_gate,
        s_up,
        s_down,
    )


def solution(mesh):
    return jax.shard_map(
        functools.partial(body, mesh.shape["ep"]),
        mesh=mesh,
        in_specs=(
            P(("grp", "ep", "tp"), None),
            P(),
            P(("grp", "ep", "tp"), None),
            P(("grp", "ep", "tp"), None),
            P("ep", None, "tp"),
            P("ep", None, "tp"),
            P("ep", "tp", None),
            P(None, "tp"),
            P(None, "tp"),
            P("tp", None),
        ),
        out_specs=P(("grp", "ep", "tp"), None),
        check_vma=False,
    )
```

time: 345 us -> 298 us (0.86)
  the two profiles are of different devices: /device:TPU:640 before, /device:TPU:513 now
where the time goes in v1:
time: 298 us
  Pallas kernels  293 us (98%)
  local copies, waits for them, and re-layouts  5.24 us (2%)
    pallas_call x1, Pallas kernels, body(): pl.pallas_call(functools.partial(kernel, n_ep, topk, cap), out_shape=jax....  293 us

profile of v1, /device:TPU:513, one launch (start us, length us, event | category | flops | bytes accessed | tf_op | source)
XLA Modules:
  0.0 298.0 jit_solution(6290607220642990676)
XLA Ops:
  0.0 1.5 copy.12.gates
  1.5 1.5 copy.11.ids
  2.9 292.7 %shard_map.100 = bf16[256,2048]{1,0:T(8,128)(2,1)} custom-call(bf16[256,2048]{1,0:T(8,128)(2,1)} %tokens.1, f32[1,2048]{1,0:T(1,128)} %bitcast.2, s32[256,2]{1,0:T(8,128)} %copy.11.ids, s32[2,256]{1,0:T(2,128)} %bitcast.3, f32[256,2]{1,0:T(8,128)} %copy.12.gates, bf16[2,2048,256]{2,1,0:T(8,128)(2,1)} %w_gate.1, bf16[2,2048,256]{2,1,0:T(8,128)(2,1)} %w_up.1, ...), custom_call_target="tpu_custom_call" | custom-call | tf_op jit(solution)/shard_map/pallas_call | solution.py:314
  295.7 2.3 copy.14

commit v2 on v1

v2 whole, which is shorter than its diff:
```python
import functools
import math

import jax
import jax.numpy as jnp
from jax import lax
from jax.experimental import pallas as pl
from jax.experimental.pallas import tpu as pltpu
from jax.sharding import PartitionSpec as P

MESH = pl.DeviceIdType.MESH
BF16, F32 = jnp.bfloat16, jnp.float32


def silu_mul(first, second):
    return first * (1.0 / (1.0 + jnp.exp(-first))) * second


def kernel(
    n_ep,
    topk,
    cap,
    tokens,
    gain,
    ids_t,
    gates_t,
    w_gate,
    w_up,
    w_down,
    s_gate,
    s_up,
    s_down,
    out,
    normed,
    packed,
    passing,
    arrived,
    results,
    passing_back,
    returned,
    total,
    wg,
    wu,
    wd,
    sg,
    su,
    sd,
    local_sem,
    w_send,
    w_recv,
    send_sem,
    recv_sem,
):
    n_rows, width = tokens.shape
    local_exp = w_gate.shape[0]
    half = w_gate.shape[2]
    experts = local_exp * n_ep
    side = math.isqrt(n_ep)
    line = side * cap
    me = lax.axis_index("ep")
    tp = lax.axis_index("tp")
    at = (lax.rem(me, side), me // side)

    def peer(axis, pos):
        return at[1] * side + pos if axis == 0 else pos * side + at[0]

    barrier = pltpu.get_barrier_semaphore()
    pl.semaphore_signal(barrier, inc=1, device_id={"tp": 1 - tp}, device_id_type=MESH)
    for axis in range(2):

        def greet(i, carry):
            to = peer(axis, lax.rem(at[axis] + i, side))
            pl.semaphore_signal(barrier, inc=1, device_id={"ep": to}, device_id_type=MESH)
            return carry

        lax.fori_loop(1, side, greet, 0)

    pairs = ((s_gate, sg), (s_up, su), (s_down, sd), (w_gate, wg), (w_up, wu), (w_down, wd))
    local = [
        pltpu.make_async_copy(src, dst.at[tp], local_sem.at[i])
        for i, (src, dst) in enumerate(pairs)
    ]
    remote = [
        pltpu.make_async_remote_copy(
            src_ref=src,
            dst_ref=dst.at[tp],
            send_sem=w_send.at[i],
            recv_sem=w_recv.at[i],
            device_id={"tp": 1 - tp},
            device_id_type=MESH,
        )
        for i, (src, dst) in enumerate(pairs)
    ]
    for copy in local:
        copy.start()

    step = min(32, n_rows)

    def norm(i, carry):
        rows = pl.ds(pl.multiple_of(i * step, step), step)
        xf = tokens[rows, :].astype(F32)
        scale = lax.rsqrt(jnp.mean(xf * xf, axis=-1, keepdims=True) + 1e-06)
        normed[rows, :] = (xf * scale * gain[...]).astype(BF16)
        return carry

    lax.fori_loop(0, n_rows // step, norm, 0)

    expert_of = lax.broadcasted_iota(jnp.int32, (experts, n_rows), 0)
    device_of, j_of = expert_of // local_exp, lax.rem(expert_of, local_exp)
    x_of, y_of = lax.rem(device_of, side), device_of // side
    flip = lax.rem(j_of, 2) == 1
    first_row = j_of * n_ep + jnp.where(flip, y_of * side + x_of, x_of * side + y_of)
    picks = [ids_t[k : k + 1, :] == expert_of for k in range(topk)]
    used = sum(p.astype(F32) for p in picks).astype(BF16)
    earlier = (
        lax.broadcasted_iota(jnp.int32, (n_rows, n_rows), 0)
        < lax.broadcasted_iota(jnp.int32, (n_rows, n_rows), 1)
    ).astype(F32).astype(BF16)
    place = jnp.dot(used, earlier, preferred_element_type=F32) + (first_row * cap).astype(F32)
    row_f = [jnp.sum(jnp.where(p, place, 0.0), axis=0, keepdims=True) for p in picks]
    row_lane = [r.astype(jnp.int32) for r in row_f]
    packed_cols = jnp.concatenate(
        row_f
        + [gates_t[k : k + 1, :] for k in range(topk)]
        + [jnp.zeros((8 - 2 * topk, n_rows), F32)],
        axis=0,
    ).T
    row_col = [packed_cols[:, k : k + 1].astype(jnp.int32) for k in range(topk)]
    gate_col = [packed_cols[:, topk + k : topk + k + 1] for k in range(topk)]

    pl.semaphore_wait(barrier, 2 * side - 1)
    for copy in remote:
        copy.start()

    def order(i):
        i = lax.rem(i + 1, side)
        return lax.rem(jnp.where(lax.rem(i, 2) == 1, (i + 1) // 2, side - i // 2), side)

    def axis_of(phase, j):
        return (j + phase + phase // 2) % 2

    def send(phase, j, pos, src, dst):
        axis = axis_of(phase, j)
        mine = at[axis]
        sem = recv_sem.at[phase, j, mine]

        @pl.when(pos == mine)
        def _():
            pltpu.make_async_copy(src, dst, sem).start()

        @pl.when(pos != mine)
        def _():
            pltpu.make_async_remote_copy(
                src_ref=src,
                dst_ref=dst,
                send_sem=send_sem.at[phase, j],
                recv_sem=sem,
                device_id={"ep": peer(axis, pos)},
                device_id_type=MESH,
            ).start()

    def arrival(phase, j, pos):
        part = packed.at[j, 0]
        pltpu.make_async_copy(part, part, recv_sem.at[phase, j, pos]).wait()

    def dispatch(i, carry):
        for j in range(local_exp):
            axis = axis_of(0, j)
            pos = lax.rem(at[axis] + order(i), side)
            row = lax.broadcasted_iota(jnp.int32, (line, n_rows), 0) + (j * side + pos) * line
            pick = functools.reduce(jnp.logical_or, [row == lane for lane in row_lane])
            pick = pick.astype(F32).astype(BF16)
            for col in range(0, width, 512):
                part = jnp.dot(pick, normed[:, col : col + 512], preferred_element_type=F32)
                packed[j, pos, :, :, col : col + 512] = part.reshape(side, cap, 512).astype(BF16)
            send(0, j, pos, packed.at[j, pos], passing.at[j, :, at[axis]])
        return carry

    lax.fori_loop(0, side, dispatch, 0)

    for copy in local:
        copy.wait()
    for copy in remote:
        copy.wait_recv()

    x = normed[...]
    parts = []
    for h in range(2):
        first = jnp.dot(x, sg[h], preferred_element_type=F32)
        second = jnp.dot(x, su[h], preferred_element_type=F32)
        parts.append(silu_mul(first, second).astype(BF16))
    hid = jnp.concatenate(parts, axis=1)

    def shared_down(n, carry):
        cols = pl.ds(pl.multiple_of(n * 256, 256), 256)
        w = sd[:, :, cols].reshape(2 * sd.shape[1], 256)
        total[:, cols] = jnp.dot(hid, w, preferred_element_type=F32)
        return carry

    lax.fori_loop(0, width // 256, shared_down, 0)

    def turn(phase, source, target):
        for j in range(local_exp):

            def landed(pos, carry):
                arrival(phase - 1, j, pos)
                return carry

            lax.fori_loop(0, side, landed, 0)
            axis = axis_of(phase, j)

            def forward(i, carry):
                pos = lax.rem(at[axis] + order(i), side)
                send(phase, j, pos, source.at[j, pos], target(j, at[axis]))
                return carry

            lax.fori_loop(0, side, forward, 0)

    turn(1, passing, lambda j, mine: arrived.at[j, mine])

    def experts_of(i, carry):
        for j in range(local_exp):
            axis = axis_of(1, j)
            pos = lax.rem(at[axis] - order(i) + side, side)
            arrival(1, j, pos)
            x = arrived[j, pos].reshape(line, width)
            parts = []
            for h in range(2):
                first = jnp.dot(x, wg[h, j], preferred_element_type=F32)
                second = jnp.dot(x, wu[h, j], preferred_element_type=F32)
                parts.append(silu_mul(first, second).astype(BF16))
            hid = jnp.concatenate(parts, axis=1)
            for col in range(0, width, 512):
                w = wd[:, j, :, col : col + 512].reshape(2 * half, 512)
                part = jnp.dot(hid, w, preferred_element_type=F32)
                results[j, pos, :, :, col : col + 512] = part.reshape(side, cap, 512).astype(BF16)
            send(2, j, pos, results.at[j, pos], passing_back.at[j, :, at[axis]])
        return carry

    lax.fori_loop(0, side, experts_of, 0)

    turn(3, passing_back, lambda j, mine: returned.at[j, mine])

    def combine(i, carry):
        weights, rows = [], []
        for j in range(local_exp):
            axis = axis_of(3, j)
            pos = lax.rem(at[axis] - order(i) + side, side)
            arrival(3, j, pos)
            row = lax.broadcasted_iota(jnp.int32, (n_rows, line), 1) + (j * side + pos) * line
            weight = sum(
                jnp.where(row == row_col[k], gate_col[k], 0.0) for k in range(topk)
            )
            high = weight.astype(BF16)
            weights += [high, (weight - high.astype(F32)).astype(BF16)]
            rows += [(j, pos)] * 2
        weights = jnp.concatenate(weights, axis=1)
        for col in range(0, width, 256):
            part = jnp.concatenate(
                [
                    returned[j, pos, :, :, col : col + 256].reshape(line, 256)
                    for j, pos in rows
                ],
                axis=0,
            )
            total[:, col : col + 256] += jnp.dot(weights, part, preferred_element_type=F32)
        return carry

    lax.fori_loop(0, side, combine, 0)

    def finish(i, carry):
        rows = pl.ds(pl.multiple_of(i * step, step), step)
        out[rows, :] = total[rows, :].astype(BF16)
        return carry

    lax.fori_loop(0, n_rows // step, finish, 0)

    for copy in remote:
        copy.wait_send()
    for phase in range(4):
        for j in range(local_exp):
            part = packed.at[j, pl.ds(0, side - 1)]
            pltpu.make_async_copy(part, part, send_sem.at[phase, j]).wait()


def body(n_ep, tokens, norm_gain, expert_ids, gate_values, w_gate, w_up, w_down, s_gate, s_up, s_down):
    n_rows, width = tokens.shape
    topk = expert_ids.shape[1]
    local_exp, _, half = w_gate.shape
    experts = local_exp * n_ep
    cap = 2 * n_rows * topk // experts
    side = math.isqrt(n_ep)
    vmem = pl.BlockSpec(memory_space=pltpu.VMEM)
    hbm = pl.BlockSpec(memory_space=pl.ANY)
    rows = pltpu.VMEM((local_exp, side, side, cap, width), BF16)
    dma = pltpu.SemaphoreType.DMA
    return pl.pallas_call(
        functools.partial(kernel, n_ep, topk, cap),
        out_shape=jax.ShapeDtypeStruct((n_rows, width), BF16),
        in_specs=[vmem] * 4 + [hbm] * 6,
        out_specs=vmem,
        scratch_shapes=[pltpu.VMEM((n_rows, width), BF16)]
        + [rows] * 6
        + [pltpu.VMEM((n_rows, width), F32)]
        + [
            pltpu.VMEM((2,) + w.shape, BF16)
            for w in (w_gate, w_up, w_down, s_gate, s_up, s_down)
        ]
        + [dma((6,))] * 3
        + [dma((4, local_exp)), dma((4, local_exp, side))],
        compiler_params=pltpu.CompilerParams(
            collective_id=0, has_side_effects=True, vmem_limit_bytes=60 * 1024 * 1024
        ),
    )(
        tokens,
        norm_gain.reshape(1, width),
        expert_ids.T,
        gate_values.T,
        w_gate,
        w_up,
        w_down,
        s_gate,
        s_up,
        s_down,
    )


def solution(mesh):
    return jax.shard_map(
        functools.partial(body, mesh.shape["ep"]),
        mesh=mesh,
        in_specs=(
            P(("grp", "ep", "tp"), None),
            P(),
            P(("grp", "ep", "tp"), None),
            P(("grp", "ep", "tp"), None),
            P("ep", None, "tp"),
            P("ep", None, "tp"),
            P("ep", "tp", None),
            P(None, "tp"),
            P(None, "tp"),
            P("tp", None),
        ),
        out_specs=P(("grp", "ep", "tp"), None),
        check_vma=False,
    )
```

time: 298 us -> 218 us (0.73)
  Pallas kernels: 293 us -> 215 us
    pallas_call x1, Pallas kernels: 293 us -> 215 us  [body(): pl.pallas_call(functools.partial(kernel, n_ep, topk, cap), out_shape=jax....]
where the time goes in v2:
time: 218 us; the launch traced here: 217 us
  Pallas kernels  215 us (99%)
  local copies, waits for them, and re-layouts  2.3 us (1%)
    pallas_call x1, Pallas kernels, body(): pl.pallas_call(functools.partial(kernel, n_ep, topk, cap), out_shape=jax....  215 us

profile of v2, /device:TPU:513, one launch (start us, length us, event | category | flops | bytes accessed | tf_op | source)
XLA Modules:
  0.0 217.4 jit_solution(5176566493430237927)
XLA Ops:
  0.0 215.1 %shard_map.100 = bf16[256,2048]{1,0:T(8,128)(2,1)} custom-call(bf16[256,2048]{1,0:T(8,128)(2,1)} %tokens.1, f32[1,2048]{1,0:T(1,128)} %bitcast.3, s32[2,256]{1,0:T(2,128)} %bitcast.4, f32[2,256]{1,0:T(2,128)} %bitcast.5, bf16[2,2048,256]{2,1,0:T(8,128)(2,1)} %w_gate.1, bf16[2,2048,256]{2,1,0:T(8,128)(2,1)} %w_up.1, bf16[2,256,2048]{2,1,0:T(8,128)(2,1)} %w_down.1, ...), custom_call_target="tpu_custom_call" | custom-call | tf_op jit(solution)/shard_map/pallas_call | solution.py:297
  215.1 2.3 %copy.12 = bf16[256,2048]{1,0:T(8,128)(2,1)} copy(bf16[256,2048]{1,0:T(8,128)(2,1)} %shard_map.100) | data formatting | bytes 2097152

commit v3 on v2

v3 whole, which is shorter than its diff:
```python
import functools
import math

import jax
import jax.numpy as jnp
from jax import lax
from jax.experimental import pallas as pl
from jax.experimental.pallas import tpu as pltpu
from jax.sharding import PartitionSpec as P

MESH = pl.DeviceIdType.MESH
BF16, F32 = jnp.bfloat16, jnp.float32


def silu_mul(first, second):
    return first * (1.0 / (1.0 + jnp.exp(-first))) * second


def kernel(
    n_ep,
    topk,
    cap,
    tokens,
    gain,
    ids_t,
    gates_t,
    w_gate,
    w_up,
    w_down,
    s_gate,
    s_up,
    s_down,
    out,
    normed,
    notes_out,
    notes_in,
    dense,
    packed,
    passing,
    arrived,
    results,
    passing_back,
    packed_back,
    sums,
    dense_back,
    total,
    wg,
    wu,
    wd,
    sg,
    su,
    sd,
    local_sem,
    w_send,
    w_recv,
    note_send,
    note_recv,
    dense_send,
    dense_recv,
    relay_send,
    relay_recv,
    cross_send,
    cross_recv,
    home_send,
    home_recv,
    hub_send,
    hub_recv,
    sum_send,
    sum_recv,
):
    n_rows, width = tokens.shape
    chunks, _, cols = normed.shape
    local_exp = w_gate.shape[0]
    half = w_gate.shape[2]
    experts = local_exp * n_ep
    side = math.isqrt(n_ep)
    line = side * cap
    reach = side // 2
    me = lax.axis_index("ep")
    tp = lax.axis_index("tp")
    at = (lax.rem(me, side), me // side)

    def peer(axis, pos):
        return at[1] * side + pos if axis == 0 else pos * side + at[0]

    def ahead(axis, s, d):
        return lax.rem(at[axis] + (d if s == 0 else side - d), side)

    def first_axis(c):
        return c % 2

    barrier = pltpu.get_barrier_semaphore()
    pl.semaphore_signal(barrier, inc=1, device_id={"tp": 1 - tp}, device_id_type=MESH)
    for axis in range(2):

        def greet(i, carry):
            to = peer(axis, lax.rem(at[axis] + i, side))
            pl.semaphore_signal(barrier, inc=1, device_id={"ep": to}, device_id_type=MESH)
            return carry

        lax.fori_loop(1, side, greet, 0)

    pairs = ((s_gate, sg), (s_up, su), (s_down, sd), (w_gate, wg), (w_up, wu), (w_down, wd))
    local = [
        pltpu.make_async_copy(src, dst.at[tp], local_sem.at[i])
        for i, (src, dst) in enumerate(pairs)
    ]
    remote = [
        pltpu.make_async_remote_copy(
            src_ref=src,
            dst_ref=dst.at[tp],
            send_sem=w_send.at[i],
            recv_sem=w_recv.at[i],
            device_id={"tp": 1 - tp},
            device_id_type=MESH,
        )
        for i, (src, dst) in enumerate(pairs)
    ]
    for copy in local:
        copy.start()

    step = min(32, n_rows)

    def norm(i, carry):
        rows = pl.ds(pl.multiple_of(i * step, step), step)
        xf = tokens[rows, :].astype(F32)
        scale = lax.rsqrt(jnp.mean(xf * xf, axis=-1, keepdims=True) + 1e-06)
        done = (xf * scale * gain[...]).astype(BF16)
        for c in range(chunks):
            normed[c, rows, :] = done[:, c * cols : (c + 1) * cols]
        return carry

    lax.fori_loop(0, n_rows // step, norm, 0)

    pl.semaphore_wait(barrier, 2 * side - 1)

    def to_peer(axis, pos, src, dst, send_sem, recv_sem):
        pltpu.make_async_remote_copy(
            src_ref=src,
            dst_ref=dst,
            send_sem=send_sem,
            recv_sem=recv_sem,
            device_id={"ep": peer(axis, pos)},
            device_id_type=MESH,
        ).start()

    def wait_for(part, sem):
        pltpu.make_async_copy(part, part, sem).wait()

    def send_dense(c):
        for s in range(2):
            axis = first_axis(c)
            to_peer(
                axis,
                ahead(axis, s, 1),
                normed.at[c],
                dense.at[c, s],
                dense_send.at[c],
                dense_recv.at[c, s],
            )

    send_dense(0)
    send_dense(1)

    expert_of = lax.broadcasted_iota(jnp.int32, (experts, n_rows), 0)
    device_of, j_of = expert_of // local_exp, lax.rem(expert_of, local_exp)
    x_of, y_of = lax.rem(device_of, side), device_of // side
    picks = [ids_t[k : k + 1, :] == expert_of for k in range(topk)]
    used = sum(p.astype(F32) for p in picks).astype(BF16)
    earlier = (
        lax.broadcasted_iota(jnp.int32, (n_rows, n_rows), 0)
        < lax.broadcasted_iota(jnp.int32, (n_rows, n_rows), 1)
    ).astype(F32).astype(BF16)
    slot = jnp.dot(used, earlier, preferred_element_type=F32)
    blank = jnp.zeros((8 - 2 * topk, n_rows), F32)
    for axis in range(2):
        pair = x_of * side + y_of if axis == 0 else y_of * side + x_of
        place = slot + ((j_of * n_ep + pair) * cap).astype(F32)
        notes_out[axis] = jnp.concatenate(
            [jnp.sum(jnp.where(p, place, 0.0), axis=0, keepdims=True) for p in picks]
            + [gates_t[k : k + 1, :] for k in range(topk)]
            + [blank],
            axis=0,
        )
    for axis in range(2):
        for s in range(2):
            to_peer(
                axis,
                ahead(axis, s, 1),
                notes_out.at[axis],
                notes_in.at[axis, s],
                note_send.at[0],
                note_recv.at[axis, s],
            )
    for c in range(2, chunks):
        send_dense(c)
    for copy in remote:
        copy.start()

    def pick_rows(notes, row):
        lanes = [notes[k : k + 1, :].astype(jnp.int32) for k in range(topk)]
        pick = functools.reduce(jnp.logical_or, [row == lane for lane in lanes])
        return pick.astype(F32).astype(BF16)

    def weigh_rows(notes, row):
        by_token = notes.T
        weight = sum(
            jnp.where(
                row == by_token[:, k : k + 1].astype(jnp.int32),
                by_token[:, topk + k : topk + k + 1],
                0.0,
            )
            for k in range(topk)
        )
        high = weight.astype(BF16)
        return high, (weight - high.astype(F32)).astype(BF16)

    tail = pl.ds(side // 2, side // 2), pl.ds(0, side // 2)
    for j in range(local_exp):
        for axis in range(2):
            row = lax.broadcasted_iota(jnp.int32, (line, n_rows), 0)
            pick = pick_rows(notes_out[axis], row + (j * side + at[axis]) * line)
            for c in range(axis, chunks, 2):
                part = jnp.dot(pick, normed[c], preferred_element_type=F32)
                passing[c, :, j, at[axis]] = part.reshape(side, cap, cols).astype(BF16)
    for c in range(chunks):
        for s in range(2):
            for j in range(local_exp):
                packed_back[c, s, reach - 2, j, tail[s]] = jnp.zeros(
                    (side // 2, cap, cols), BF16
                )

    parts_of = (pl.ds(0, side // 2), pl.ds(side // 2, side // 2))

    def relay(j, c):
        axis = first_axis(c)
        for s in range(2):
            if j == 0:
                wait_for(dense.at[c, s], dense_recv.at[c, s])
                if c < 2:
                    wait_for(notes_in.at[axis, s], note_recv.at[axis, s])
            source = ahead(axis, 1 - s, 1)
            i = lax.broadcasted_iota(jnp.int32, (reach * line, n_rows), 0)
            d = i // line
            pos = lax.rem(at[axis] + (d if s == 0 else side - d), side)
            row = (j * side + pos) * line + lax.rem(i, line)
            pick = pick_rows(notes_in[axis, s], row)
            part = jnp.dot(pick, dense[c, s], preferred_element_type=F32).astype(BF16)
            part = part.reshape(reach, side, cap, cols)
            packed[c, j, s] = part[1:]
            passing[c, :, j, source] = part[0]
            for d in range(1, reach):
                rows = pl.ds(0, side) if d < reach - 1 else parts_of[s]
                to_peer(
                    axis,
                    ahead(axis, s, d),
                    packed.at[c, j, s, d - 1, rows],
                    passing.at[c, rows, j, source],
                    relay_send.at[c, j],
                    relay_recv.at[c, j],
                )

    for j in range(local_exp):
        for c in range(chunks):
            relay(j, c)

    for copy in local:
        copy.wait()
    for copy in remote:
        copy.wait_recv()
    parts = []
    for h in range(2):
        first = sum(
            jnp.dot(normed[c], sg[h, c * cols : (c + 1) * cols], preferred_element_type=F32)
            for c in range(chunks)
        )
        second = sum(
            jnp.dot(normed[c], su[h, c * cols : (c + 1) * cols], preferred_element_type=F32)
            for c in range(chunks)
        )
        parts.append(silu_mul(first, second).astype(BF16))
    hid = jnp.concatenate(parts, axis=1)
    for c in range(chunks):
        w = sd[:, :, c * cols : (c + 1) * cols].reshape(2 * half, cols)
        total[c] = jnp.dot(hid, w, preferred_element_type=F32)

    def order(i):
        i = lax.rem(i + 1, side)
        return lax.rem(jnp.where(lax.rem(i, 2) == 1, (i + 1) // 2, side - i // 2), side)

    def across(j, c, source_of, target_of, send_sem, recv_sem):
        axis = 1 - first_axis(c)
        mine = at[axis]

        def one(i, carry):
            pos = lax.rem(mine + order(i), side)
            src, dst = source_of(pos), target_of(mine)

            @pl.when(pos == mine)
            def _():
                pltpu.make_async_copy(src, dst, recv_sem.at[c, j]).start()

            @pl.when(pos != mine)
            def _():
                to_peer(axis, pos, src, dst, send_sem.at[c, j], recv_sem.at[c, j])

            return carry

        lax.fori_loop(0, side, one, 0)

    def by_source(ref, j, c, pos):
        return ref.at[c, j, pos] if first_axis(c) == 0 else ref.at[c, j, :, pos]

    for j in range(local_exp):
        for c in range(chunks):
            wait_for(results.at[c, 0, pl.ds(0, side - 3)], relay_recv.at[c, j])
            across(
                j,
                c,
                lambda pos: passing.at[c, pos, j],
                lambda mine: by_source(arrived, j, c, mine),
                cross_send,
                cross_recv,
            )

    block = max(1, side // 2)
    for j in range(local_exp):
        for c in range(chunks):
            wait_for(results.at[c, 0], cross_recv.at[c, j])

        def experts_of(i, carry):
            rows = pl.ds(i * block, block)
            xs = [
                arrived[c, j, rows].reshape(block * line, cols) for c in range(chunks)
            ]
            parts = []
            for h in range(2):
                first = sum(
                    jnp.dot(xs[c], wg[h, j, c * cols : (c + 1) * cols], preferred_element_type=F32)
                    for c in range(chunks)
                )
                second = sum(
                    jnp.dot(xs[c], wu[h, j, c * cols : (c + 1) * cols], preferred_element_type=F32)
                    for c in range(chunks)
                )
                parts.append(silu_mul(first, second).astype(BF16))
            hid = jnp.concatenate(parts, axis=1)
            for c in range(chunks):
                w = wd[:, j, :, c * cols : (c + 1) * cols].reshape(2 * half, cols)
                part = jnp.dot(hid, w, preferred_element_type=F32)
                results[c, j, rows] = part.reshape(block, side, cap, cols).astype(BF16)
            return carry

        lax.fori_loop(0, side // block, experts_of, 0)
        for c in range(chunks):
            across(
                j,
                c,
                lambda pos: by_source(results, j, c, pos),
                lambda mine: passing_back.at[c, j, :, mine],
                home_send,
                home_recv,
            )

    for j in range(local_exp):
        for c in range(chunks):
            axis = first_axis(c)
            wait_for(results.at[c, 0], home_recv.at[c, j])
            for d in range(1, reach):
                for s in range(2):
                    rows = pl.ds(0, side) if d < reach - 1 else parts_of[s]
                    to_peer(
                        axis,
                        ahead(axis, 1 - s, d),
                        passing_back.at[c, j, ahead(axis, 1 - s, d + 1), rows],
                        packed_back.at[c, s, d - 1, j, rows],
                        hub_send.at[c, j],
                        hub_recv.at[c, s],
                    )

    for axis in range(2):
        i = lax.broadcasted_iota(jnp.int32, (n_rows, local_exp * line), 1)
        row = (i // line * side + at[axis]) * line + lax.rem(i, line)
        high, low = weigh_rows(notes_out[axis], row)
        for c in range(axis, chunks, 2):
            rhs = jnp.concatenate(
                [passing_back[c, j, at[axis]].reshape(line, cols) for j in range(local_exp)], axis=0
            )
            total[c] += jnp.dot(high, rhs, preferred_element_type=F32) + jnp.dot(
                low, rhs, preferred_element_type=F32
            )

    for c in range(chunks):
        axis = first_axis(c)
        for s in range(2):
            source = ahead(axis, 1 - s, 1)
            i = lax.broadcasted_iota(jnp.int32, (n_rows, reach * local_exp * line), 1)
            d = i // (local_exp * line)
            j_row = lax.rem(i // line, local_exp)
            pos = lax.rem(at[axis] + (d if s == 0 else side - d), side)
            row = (j_row * side + pos) * line + lax.rem(i, line)
            high, low = weigh_rows(notes_in[axis, s], row)
            wait_for(results.at[c, 0, pl.ds(0, side - 3)], hub_recv.at[c, s])
            rhs = jnp.concatenate(
                [passing_back[c, j, source].reshape(line, cols) for j in range(local_exp)]
                + [packed_back[c, s].reshape((reach - 1) * local_exp * line, cols)],
                axis=0,
            )
            part = jnp.dot(high, rhs, preferred_element_type=F32) + jnp.dot(
                low, rhs, preferred_element_type=F32
            )
            sums[c, s] = part.astype(BF16)
            to_peer(
                axis,
                source,
                sums.at[c, s],
                dense_back.at[c, 1 - s],
                sum_send.at[c],
                sum_recv.at[c, 1 - s],
            )

    for c in range(chunks):
        for s in range(2):
            wait_for(dense_back.at[c, s], sum_recv.at[c, s])
        mixed = total[c] + dense_back[c, 0].astype(F32) + dense_back[c, 1].astype(F32)
        out[:, c * cols : (c + 1) * cols] = mixed.astype(BF16)

    for copy in remote:
        copy.wait_send()
    wait_for(notes_in, note_send.at[0])
    for c in range(chunks):
        wait_for(dense.at[c], dense_send.at[c])
        wait_for(sums.at[c], sum_send.at[c])
        for j in range(local_exp):
            wait_for(results.at[c, 0, pl.ds(0, side - 3)], relay_send.at[c, j])
            wait_for(results.at[c, 0, pl.ds(0, side - 1)], cross_send.at[c, j])
            wait_for(results.at[c, 0, pl.ds(0, side - 1)], home_send.at[c, j])
            wait_for(results.at[c, 0, pl.ds(0, side - 3)], hub_send.at[c, j])


def body(n_ep, tokens, norm_gain, expert_ids, gate_values, w_gate, w_up, w_down, s_gate, s_up, s_down):
    n_rows, width = tokens.shape
    topk = expert_ids.shape[1]
    local_exp, _, half = w_gate.shape
    experts = local_exp * n_ep
    cap = 2 * n_rows * topk // experts
    side = math.isqrt(n_ep)
    chunks = 4
    cols = width // chunks
    reach = side // 2
    vmem = pl.BlockSpec(memory_space=pltpu.VMEM)
    hbm = pl.BlockSpec(memory_space=pl.ANY)
    dma = pltpu.SemaphoreType.DMA

    def tall(*shape):
        return pltpu.VMEM((chunks,) + shape + (cols,), BF16)

    per_expert, per_side = dma((chunks, local_exp)), dma((chunks, 2))
    return pl.pallas_call(
        functools.partial(kernel, n_ep, topk, cap),
        out_shape=jax.ShapeDtypeStruct((n_rows, width), BF16),
        in_specs=[vmem] * 4 + [hbm] * 6,
        out_specs=vmem,
        scratch_shapes=[
            tall(n_rows),
            pltpu.VMEM((2, 8, n_rows), F32),
            pltpu.VMEM((2, 2, 8, n_rows), F32),
            tall(2, n_rows),
            tall(local_exp, 2, reach - 1, side, cap),
            tall(side, local_exp, side, cap),
            tall(local_exp, side, side, cap),
            tall(local_exp, side, side, cap),
            tall(local_exp, side, side, cap),
            tall(2, reach - 1, local_exp, side, cap),
            tall(2, n_rows),
            tall(2, n_rows),
            pltpu.VMEM((chunks, n_rows, cols), F32),
        ]
        + [
            pltpu.VMEM((2,) + w.shape, BF16)
            for w in (w_gate, w_up, w_down, s_gate, s_up, s_down)
        ]
        + [dma((6,))] * 3
        + [dma((1,)), dma((2, 2)), dma((chunks,)), per_side]
        + [per_expert] * 6
        + [per_expert, per_side, dma((chunks,)), per_side],
        compiler_params=pltpu.CompilerParams(
            collective_id=0, has_side_effects=True, vmem_limit_bytes=62 * 1024 * 1024
        ),
    )(
        tokens,
        norm_gain.reshape(1, width),
        expert_ids.T,
        gate_values.T,
        w_gate,
        w_up,
        w_down,
        s_gate,
        s_up,
        s_down,
    )


def solution(mesh):
    return jax.shard_map(
        functools.partial(body, mesh.shape["ep"]),
        mesh=mesh,
        in_specs=(
            P(("grp", "ep", "tp"), None),
            P(),
            P(("grp", "ep", "tp"), None),
            P(("grp", "ep", "tp"), None),
            P("ep", None, "tp"),
            P("ep", None, "tp"),
            P("ep", "tp", None),
            P(None, "tp"),
            P(None, "tp"),
            P("tp", None),
        ),
        out_specs=P(("grp", "ep", "tp"), None),
        check_vma=False,
    )
```

time: 218 us -> 190 us (0.87)
  Pallas kernels: 215 us -> 186 us
    pallas_call x1, Pallas kernels: 215 us -> 186 us  [body(): pl.pallas_call(functools.partial(kernel, n_ep, topk, cap), out_shape=jax....]
where the time goes in v3:
time: 190 us; the launch traced here: 188 us
  Pallas kernels  186 us (98%)
  local copies, waits for them, and re-layouts  2.3 us (1%)
    pallas_call x1, Pallas kernels, body(): pl.pallas_call(functools.partial(kernel, n_ep, topk, cap), out_shape=jax....  186 us

profile of v3, /device:TPU:513, one launch (start us, length us, event | category | flops | bytes accessed | tf_op | source)
XLA Modules:
  0.0 188.3 jit_solution(4335952494539525247)
XLA Ops:
  0.0 186.0 %shard_map.100 = bf16[256,2048]{1,0:T(8,128)(2,1)} custom-call(bf16[256,2048]{1,0:T(8,128)(2,1)} %tokens.1, f32[1,2048]{1,0:T(1,128)} %bitcast.3, s32[2,256]{1,0:T(2,128)} %bitcast.4, f32[2,256]{1,0:T(2,128)} %bitcast.5, bf16[2,2048,256]{2,1,0:T(8,128)(2,1)} %w_gate.1, bf16[2,2048,256]{2,1,0:T(8,128)(2,1)} %w_up.1, bf16[2,256,2048]{2,1,0:T(8,128)(2,1)} %w_down.1, ...), custom_call_target="tpu_custom_call" | custom-call | tf_op jit(solution)/shard_map/pallas_call | solution.py:459
  186.0 2.3 %copy.12 = bf16[256,2048]{1,0:T(8,128)(2,1)} copy(bf16[256,2048]{1,0:T(8,128)(2,1)} %shard_map.100) | data formatting | bytes 2097152

commit v4 on v3

--- a/solution.py
+++ b/solution.py
@@ -10,6 +10,7 @@
 
 MESH = pl.DeviceIdType.MESH
 BF16, F32 = jnp.bfloat16, jnp.float32
+VMEM_MIB = 62
 
 
 def silu_mul(first, second):
@@ -35,13 +36,13 @@
     notes_out,
     notes_in,
     dense,
+    dense_far,
     packed,
     passing,
     arrived,
-    results,
     passing_back,
     packed_back,
-    sums,
+    chain,
     dense_back,
     total,
     wg,
@@ -57,6 +58,8 @@
     note_recv,
     dense_send,
     dense_recv,
+    far_send,
+    far_recv,
     relay_send,
     relay_recv,
     cross_send,
@@ -65,6 +68,8 @@
     home_recv,
     hub_send,
     hub_recv,
+    chain_send,
+    chain_recv,
     sum_send,
     sum_recv,
 ):
@@ -75,7 +80,8 @@
     experts = local_exp * n_ep
     side = math.isqrt(n_ep)
     line = side * cap
-    reach = side // 2
+    reach = side // 2 - 1
+    relayed = max(0, 2 * reach - 3)
     me = lax.axis_index("ep")
     tp = lax.axis_index("tp")
     at = (lax.rem(me, side), me // side)
@@ -88,6 +94,11 @@
 
     def first_axis(c):
         return c % 2
+
+    def span(distance, s):
+        if distance < side // 2:
+            return pl.ds(0, side)
+        return pl.ds(s * (side // 2), side // 2)
 
     barrier = pltpu.get_barrier_semaphore()
     pl.semaphore_signal(barrier, inc=1, device_id={"tp": 1 - tp}, device_id_type=MESH)
@@ -119,19 +130,6 @@
     for copy in local:
         copy.start()
 
-    step = min(32, n_rows)
-
-    def norm(i, carry):
-        rows = pl.ds(pl.multiple_of(i * step, step), step)
-        xf = tokens[rows, :].astype(F32)
-        scale = lax.rsqrt(jnp.mean(xf * xf, axis=-1, keepdims=True) + 1e-06)
-        done = (xf * scale * gain[...]).astype(BF16)
-        for c in range(chunks):
-            normed[c, rows, :] = done[:, c * cols : (c + 1) * cols]
-        return carry
-
-    lax.fori_loop(0, n_rows // step, norm, 0)
-
     pl.semaphore_wait(barrier, 2 * side - 1)
 
     def to_peer(axis, pos, src, dst, send_sem, recv_sem):
@@ -153,7 +151,7 @@
             to_peer(
                 axis,
                 ahead(axis, s, 1),
-                normed.at[c],
+                tokens.at[:, c * cols : (c + 1) * cols],
                 dense.at[c, s],
                 dense_send.at[c],
                 dense_recv.at[c, s],
@@ -184,14 +182,15 @@
         )
     for axis in range(2):
         for s in range(2):
-            to_peer(
-                axis,
-                ahead(axis, s, 1),
-                notes_out.at[axis],
-                notes_in.at[axis, s],
-                note_send.at[0],
-                note_recv.at[axis, s],
-            )
+            for far in range(2):
+                to_peer(
+                    axis,
+                    ahead(axis, s, far + 1),
+                    notes_out.at[axis],
+                    notes_in.at[axis, s, far],
+                    note_send.at[0],
+                    note_recv.at[axis, s, far],
+                )
     for c in range(2, chunks):
         send_dense(c)
     for copy in remote:
@@ -215,42 +214,69 @@
         high = weight.astype(BF16)
         return high, (weight - high.astype(F32)).astype(BF16)
 
-    tail = pl.ds(side // 2, side // 2), pl.ds(0, side // 2)
-    for j in range(local_exp):
-        for axis in range(2):
-            row = lax.broadcasted_iota(jnp.int32, (line, n_rows), 0)
-            pick = pick_rows(notes_out[axis], row + (j * side + at[axis]) * line)
-            for c in range(axis, chunks, 2):
-                part = jnp.dot(pick, normed[c], preferred_element_type=F32)
-                passing[c, :, j, at[axis]] = part.reshape(side, cap, cols).astype(BF16)
+    def pick_own(notes, axis):
+        i = lax.broadcasted_iota(jnp.int32, (local_exp * line, n_rows), 0)
+        row = (i // line * side + at[axis]) * line + lax.rem(i, line)
+        return pick_rows(notes, row)
+
+    def keep_own(pick, source, pos, c):
+        part = jnp.dot(pick, source, preferred_element_type=F32).astype(BF16)
+        part = part.reshape(local_exp, side, cap, cols)
+        for j in range(local_exp):
+            passing[c, :, j, pos] = part[j]
+
+    for axis in range(2):
+        pick = pick_own(notes_out[axis], axis)
+        for c in range(axis, chunks, 2):
+            part = tokens[:, c * cols : (c + 1) * cols]
+            keep_own(pick, part, at[axis], c)
+    if reach > 1:
+        for c in range(chunks):
+            for s in range(2):
+                for j in range(local_exp):
+                    packed_back[c, s, reach - 2, j, span(side // 2, 1 - s)] = jnp.zeros(
+                        (side // 2, cap, cols), BF16
+                    )
+
     for c in range(chunks):
-        for s in range(2):
-            for j in range(local_exp):
-                packed_back[c, s, reach - 2, j, tail[s]] = jnp.zeros(
-                    (side // 2, cap, cols), BF16
-                )
-
-    parts_of = (pl.ds(0, side // 2), pl.ds(side // 2, side // 2))
+        axis = first_axis(c)
+        for s in range(2):
+            wait_for(dense.at[c, s], dense_recv.at[c, s])
+            to_peer(
+                axis,
+                ahead(axis, s, 1),
+                dense.at[c, s],
+                dense_far.at[c, s],
+                far_send.at[c],
+                far_recv.at[c, s],
+            )
+        for s in range(2):
+            if c < 2:
+                wait_for(notes_in.at[axis, s, 0], note_recv.at[axis, s, 0])
+            pick = pick_own(notes_in[axis, s, 0], axis)
+            keep_own(pick, dense[c, s], ahead(axis, 1 - s, 1), c)
 
     def relay(j, c):
         axis = first_axis(c)
         for s in range(2):
             if j == 0:
-                wait_for(dense.at[c, s], dense_recv.at[c, s])
+                wait_for(dense_far.at[c, s], far_recv.at[c, s])
                 if c < 2:
-                    wait_for(notes_in.at[axis, s], note_recv.at[axis, s])
-            source = ahead(axis, 1 - s, 1)
+                    wait_for(notes_in.at[axis, s, 1], note_recv.at[axis, s, 1])
+            source = ahead(axis, 1 - s, 2)
             i = lax.broadcasted_iota(jnp.int32, (reach * line, n_rows), 0)
             d = i // line
             pos = lax.rem(at[axis] + (d if s == 0 else side - d), side)
             row = (j * side + pos) * line + lax.rem(i, line)
-            pick = pick_rows(notes_in[axis, s], row)
-            part = jnp.dot(pick, dense[c, s], preferred_element_type=F32).astype(BF16)
+            pick = pick_rows(notes_in[axis, s, 1], row)
+            part = jnp.dot(pick, dense_far[c, s], preferred_element_type=F32).astype(BF16)
             part = part.reshape(reach, side, cap, cols)
-            packed[c, j, s] = part[1:]
-            passing[c, :, j, source] = part[0]
+            if reach > 1:
+                packed[c, j, s] = part[1:]
+            rows = span(2, s)
+            passing[c, rows, j, source] = part[0, rows.start : rows.start + rows.size]
             for d in range(1, reach):
-                rows = pl.ds(0, side) if d < reach - 1 else parts_of[s]
+                rows = span(d + 2, s)
                 to_peer(
                     axis,
                     ahead(axis, s, d),
@@ -264,6 +290,24 @@
         for c in range(chunks):
             relay(j, c)
 
+    step = min(32, n_rows)
+
+    def scaled(parts):
+        square = sum(jnp.sum(p * p, axis=-1, keepdims=True) for p in parts)
+        scale = lax.rsqrt(square * (1.0 / width) + 1e-06)
+        return [
+            (p * scale * gain[:, c * cols : (c + 1) * cols]).astype(BF16)
+            for c, p in enumerate(parts)
+        ]
+
+    def norm(i, carry):
+        rows = pl.ds(pl.multiple_of(i * step, step), step)
+        parts = [tokens[rows, c * cols : (c + 1) * cols].astype(F32) for c in range(chunks)]
+        for c, part in enumerate(scaled(parts)):
+            normed[c, rows, :] = part
+        return carry
+
+    lax.fori_loop(0, n_rows // step, norm, 0)
     for copy in local:
         copy.wait()
     for copy in remote:
@@ -313,7 +357,8 @@
 
     for j in range(local_exp):
         for c in range(chunks):
-            wait_for(results.at[c, 0, pl.ds(0, side - 3)], relay_recv.at[c, j])
+            if relayed:
+                wait_for(arrived.at[c, 0, pl.ds(0, relayed)], relay_recv.at[c, j])
             across(
                 j,
                 c,
@@ -326,7 +371,15 @@
     block = max(1, side // 2)
     for j in range(local_exp):
         for c in range(chunks):
-            wait_for(results.at[c, 0], cross_recv.at[c, j])
+            wait_for(arrived.at[c, 0], cross_recv.at[c, j])
+
+        def norm_rows(i, carry):
+            parts = [arrived[c, j, i].reshape(line, cols).astype(F32) for c in range(chunks)]
+            for c, part in enumerate(scaled(parts)):
+                arrived[c, j, i] = part.reshape(side, cap, cols)
+            return carry
+
+        lax.fori_loop(0, side, norm_rows, 0)
 
         def experts_of(i, carry):
             rows = pl.ds(i * block, block)
@@ -348,7 +401,7 @@
             for c in range(chunks):
                 w = wd[:, j, :, c * cols : (c + 1) * cols].reshape(2 * half, cols)
                 part = jnp.dot(hid, w, preferred_element_type=F32)
-                results[c, j, rows] = part.reshape(block, side, cap, cols).astype(BF16)
+                arrived[c, j, rows] = part.reshape(block, side, cap, cols).astype(BF16)
             return carry
 
         lax.fori_loop(0, side // block, experts_of, 0)
@@ -356,7 +409,7 @@
             across(
                 j,
                 c,
-                lambda pos: by_source(results, j, c, pos),
+                lambda pos: by_source(arrived, j, c, pos),
                 lambda mine: passing_back.at[c, j, :, mine],
                 home_send,
                 home_recv,
@@ -365,55 +418,77 @@
     for j in range(local_exp):
         for c in range(chunks):
             axis = first_axis(c)
-            wait_for(results.at[c, 0], home_recv.at[c, j])
+            wait_for(arrived.at[c, 0], home_recv.at[c, j])
             for d in range(1, reach):
                 for s in range(2):
-                    rows = pl.ds(0, side) if d < reach - 1 else parts_of[s]
+                    rows = span(d + 2, s)
                     to_peer(
                         axis,
                         ahead(axis, 1 - s, d),
-                        passing_back.at[c, j, ahead(axis, 1 - s, d + 1), rows],
+                        passing_back.at[c, j, ahead(axis, 1 - s, d + 2), rows],
                         packed_back.at[c, s, d - 1, j, rows],
                         hub_send.at[c, j],
                         hub_recv.at[c, s],
                     )
 
+    def weigh_own(notes, axis):
+        i = lax.broadcasted_iota(jnp.int32, (1, local_exp * line), 1)
+        row = (i // line * side + at[axis]) * line + lax.rem(i, line)
+        return weigh_rows(notes, row)
+
+    def own_rows(c, pos):
+        return [passing_back[c, j, pos].reshape(line, cols) for j in range(local_exp)]
+
+    def product(weights, rows):
+        rows = jnp.concatenate(rows, axis=0)
+        return sum(jnp.dot(w, rows, preferred_element_type=F32) for w in weights)
+
     for axis in range(2):
-        i = lax.broadcasted_iota(jnp.int32, (n_rows, local_exp * line), 1)
-        row = (i // line * side + at[axis]) * line + lax.rem(i, line)
-        high, low = weigh_rows(notes_out[axis], row)
+        weights = weigh_own(notes_out[axis], axis)
         for c in range(axis, chunks, 2):
-            rhs = jnp.concatenate(
-                [passing_back[c, j, at[axis]].reshape(line, cols) for j in range(local_exp)], axis=0
-            )
-            total[c] += jnp.dot(high, rhs, preferred_element_type=F32) + jnp.dot(
-                low, rhs, preferred_element_type=F32
-            )
+            total[c] += product(weights, own_rows(c, at[axis]))
 
     for c in range(chunks):
         axis = first_axis(c)
-        for s in range(2):
-            source = ahead(axis, 1 - s, 1)
-            i = lax.broadcasted_iota(jnp.int32, (n_rows, reach * local_exp * line), 1)
+        wait_for(dense.at[c], far_send.at[c])
+        for s in range(2):
+            i = lax.broadcasted_iota(jnp.int32, (1, reach * local_exp * line), 1)
             d = i // (local_exp * line)
             j_row = lax.rem(i // line, local_exp)
             pos = lax.rem(at[axis] + (d if s == 0 else side - d), side)
             row = (j_row * side + pos) * line + lax.rem(i, line)
-            high, low = weigh_rows(notes_in[axis, s], row)
-            wait_for(results.at[c, 0, pl.ds(0, side - 3)], hub_recv.at[c, s])
-            rhs = jnp.concatenate(
-                [passing_back[c, j, source].reshape(line, cols) for j in range(local_exp)]
-                + [packed_back[c, s].reshape((reach - 1) * local_exp * line, cols)],
-                axis=0,
+            mine = span(side // 2, s)
+            second = lax.rem(i, line) // cap
+            inside = (second >= mine.start) & (second < mine.start + mine.size)
+            row = jnp.where((d < reach - 1) | inside, row, -1)
+            weights = weigh_rows(notes_in[axis, s, 1], row)
+            rows = own_rows(c, ahead(axis, 1 - s, 2))
+            if reach > 1:
+                wait_for(
+                    arrived.at[c, 0, pl.ds(0, relayed * local_exp // 2)], hub_recv.at[c, s]
+                )
+                rows += [packed_back[c, s].reshape((reach - 1) * local_exp * line, cols)]
+            dense_far[c, s] = product(weights, rows).astype(BF16)
+            to_peer(
+                axis,
+                ahead(axis, 1 - s, 1),
+                dense_far.at[c, s],
+                chain.at[c, s],
+                chain_send.at[c],
+                chain_recv.at[c, s],
             )
-            part = jnp.dot(high, rhs, preferred_element_type=F32) + jnp.dot(
-                low, rhs, preferred_element_type=F32
-            )
-            sums[c, s] = part.astype(BF16)
+
+    for c in range(chunks):
+        axis = first_axis(c)
+        for s in range(2):
+            source = ahead(axis, 1 - s, 1)
+            part = product(weigh_own(notes_in[axis, s, 0], axis), own_rows(c, source))
+            wait_for(chain.at[c, s], chain_recv.at[c, s])
+            dense[c, s] = (part + chain[c, s].astype(F32)).astype(BF16)
             to_peer(
                 axis,
                 source,
-                sums.at[c, s],
+                dense.at[c, s],
                 dense_back.at[c, 1 - s],
                 sum_send.at[c],
                 sum_recv.at[c, 1 - s],
@@ -430,12 +505,14 @@
     wait_for(notes_in, note_send.at[0])
     for c in range(chunks):
         wait_for(dense.at[c], dense_send.at[c])
-        wait_for(sums.at[c], sum_send.at[c])
+        wait_for(dense.at[c], chain_send.at[c])
+        wait_for(dense.at[c], sum_send.at[c])
         for j in range(local_exp):
-            wait_for(results.at[c, 0, pl.ds(0, side - 3)], relay_send.at[c, j])
-            wait_for(results.at[c, 0, pl.ds(0, side - 1)], cross_send.at[c, j])
-            wait_for(results.at[c, 0, pl.ds(0, side - 1)], home_send.at[c, j])
-            wait_for(results.at[c, 0, pl.ds(0, side - 3)], hub_send.at[c, j])
+            wait_for(arrived.at[c, 0, pl.ds(0, side - 1)], cross_send.at[c, j])
+            wait_for(arrived.at[c, 0, pl.ds(0, side - 1)], home_send.at[c, j])
+            if relayed:
+                wait_for(arrived.at[c, 0, pl.ds(0, relayed)], relay_send.at[c, j])
+                wait_for(arrived.at[c, 0, pl.ds(0, relayed)], hub_send.at[c, j])
 
 
 def body(n_ep, tokens, norm_gain, expert_ids, gate_values, w_gate, w_up, w_down, s_gate, s_up, s_down):
@@ -447,7 +524,7 @@
     side = math.isqrt(n_ep)
     chunks = 4
     cols = width // chunks
-    reach = side // 2
+    reach = side // 2 - 1
     vmem = pl.BlockSpec(memory_space=pltpu.VMEM)
     hbm = pl.BlockSpec(memory_space=pl.ANY)
     dma = pltpu.SemaphoreType.DMA
@@ -464,14 +541,14 @@
         scratch_shapes=[
             tall(n_rows),
             pltpu.VMEM((2, 8, n_rows), F32),
-            pltpu.VMEM((2, 2, 8, n_rows), F32),
+            pltpu.VMEM((2, 2, 2, 8, n_rows), F32),
             tall(2, n_rows),
-            tall(local_exp, 2, reach - 1, side, cap),
+            tall(2, n_rows),
+            tall(local_exp, 2, max(1, reach - 1), side, cap),
             tall(side, local_exp, side, cap),
             tall(local_exp, side, side, cap),
             tall(local_exp, side, side, cap),
-            tall(local_exp, side, side, cap),
-            tall(2, reach - 1, local_exp, side, cap),
+            tall(2, max(1, reach - 1), local_exp, side, cap),
             tall(2, n_rows),
             tall(2, n_rows),
             pltpu.VMEM((chunks, n_rows, cols), F32),
@@ -481,11 +558,13 @@
             for w in (w_gate, w_up, w_down, s_gate, s_up, s_down)
         ]
         + [dma((6,))] * 3
-        + [dma((1,)), dma((2, 2)), dma((chunks,)), per_side]
-        + [per_expert] * 6
-        + [per_expert, per_side, dma((chunks,)), per_side],
+        + [dma((1,)), dma((2, 2, 2))]
+        + [dma((chunks,)), per_side] * 2
+        + [per_expert] * 7
+        + [per_side]
+        + [dma((chunks,)), per_side] * 2,
         compiler_params=pltpu.CompilerParams(
-            collective_id=0, has_side_effects=True, vmem_limit_bytes=62 * 1024 * 1024
+            collective_id=0, has_side_effects=True, vmem_limit_bytes=VMEM_MIB * 1024 * 1024
         ),
     )(
         tokens,

time: 190 us -> 185 us (0.974)
  Pallas kernels: 186 us -> 183 us
    pallas_call x1, Pallas kernels: 186 us -> 183 us  [body(): pl.pallas_call(functools.partial(kernel, n_ep, topk, cap), out_shape=jax....]
where the time goes in v4:
time: 185 us
  Pallas kernels  183 us (99%)
  local copies, waits for them, and re-layouts  2.3 us (1%)
    pallas_call x1, Pallas kernels, body(): pl.pallas_call(functools.partial(kernel, n_ep, topk, cap), out_shape=jax....  183 us

profile of v4, /device:TPU:513, one launch (start us, length us, event | category | flops | bytes accessed | tf_op | source)
XLA Modules:
  0.0 185.0 jit_solution(7652157804898243561)
XLA Ops:
  0.0 182.7 %shard_map.100 = bf16[256,2048]{1,0:T(8,128)(2,1)} custom-call(bf16[256,2048]{1,0:T(8,128)(2,1)} %tokens.1, f32[1,2048]{1,0:T(1,128)} %bitcast.3, s32[2,256]{1,0:T(2,128)} %bitcast.4, f32[2,256]{1,0:T(2,128)} %bitcast.5, bf16[2,2048,256]{2,1,0:T(8,128)(2,1)} %w_gate.1, bf16[2,2048,256]{2,1,0:T(8,128)(2,1)} %w_up.1, bf16[2,256,2048]{2,1,0:T(8,128)(2,1)} %w_down.1, ...), custom_call_target="tpu_custom_call" | custom-call | tf_op jit(solution)/shard_map/pallas_call | solution.py:536
  182.7 2.3 %copy.12 = bf16[256,2048]{1,0:T(8,128)(2,1)} copy(bf16[256,2048]{1,0:T(8,128)(2,1)} %shard_map.100) | data formatting | bytes 2097152

commit v5 on v4

--- a/solution.py
+++ b/solution.py
@@ -21,10 +21,10 @@
     n_ep,
     topk,
     cap,
-    tokens,
-    gain,
-    ids_t,
-    gates_t,
+    tokens_in,
+    gain_in,
+    ids_in,
+    gates_in,
     w_gate,
     w_up,
     w_down,
@@ -32,6 +32,10 @@
     s_up,
     s_down,
     out,
+    tokens,
+    gain,
+    ids_t,
+    gates_t,
     normed,
     notes_out,
     notes_in,
@@ -51,6 +55,8 @@
     sg,
     su,
     sd,
+    small_sem,
+    token_sem,
     local_sem,
     w_send,
     w_recv,
@@ -73,8 +79,8 @@
     sum_send,
     sum_recv,
 ):
-    n_rows, width = tokens.shape
-    chunks, _, cols = normed.shape
+    chunks, n_rows, cols = tokens.shape
+    width = chunks * cols
     local_exp = w_gate.shape[0]
     half = w_gate.shape[2]
     experts = local_exp * n_ep
@@ -127,7 +133,17 @@
         )
         for i, (src, dst) in enumerate(pairs)
     ]
-    for copy in local:
+    token_loads = [
+        pltpu.make_async_copy(
+            tokens_in.at[:, c * cols : (c + 1) * cols], tokens.at[c], token_sem.at[c]
+        )
+        for c in range(chunks)
+    ]
+    small_loads = [
+        pltpu.make_async_copy(src, dst, small_sem.at[i])
+        for i, (src, dst) in enumerate(((ids_in, ids_t), (gates_in, gates_t), (gain_in, gain)))
+    ]
+    for copy in token_loads[:2] + small_loads + token_loads[2:] + local:
         copy.start()
 
     pl.semaphore_wait(barrier, 2 * side - 1)
@@ -146,12 +162,13 @@
         pltpu.make_async_copy(part, part, sem).wait()
 
     def send_dense(c):
+        token_loads[c].wait()
         for s in range(2):
             axis = first_axis(c)
             to_peer(
                 axis,
                 ahead(axis, s, 1),
-                tokens.at[:, c * cols : (c + 1) * cols],
+                tokens.at[c],
                 dense.at[c, s],
                 dense_send.at[c],
                 dense_recv.at[c, s],
@@ -159,6 +176,9 @@
 
     send_dense(0)
     send_dense(1)
+
+    for copy in small_loads:
+        copy.wait()
 
     expert_of = lax.broadcasted_iota(jnp.int32, (experts, n_rows), 0)
     device_of, j_of = expert_of // local_exp, lax.rem(expert_of, local_exp)
@@ -228,8 +248,7 @@
     for axis in range(2):
         pick = pick_own(notes_out[axis], axis)
         for c in range(axis, chunks, 2):
-            part = tokens[:, c * cols : (c + 1) * cols]
-            keep_own(pick, part, at[axis], c)
+            keep_own(pick, tokens[c], at[axis], c)
     if reach > 1:
         for c in range(chunks):
             for s in range(2):
@@ -302,7 +321,7 @@
 
     def norm(i, carry):
         rows = pl.ds(pl.multiple_of(i * step, step), step)
-        parts = [tokens[rows, c * cols : (c + 1) * cols].astype(F32) for c in range(chunks)]
+        parts = [tokens[c, rows, :].astype(F32) for c in range(chunks)]
         for c, part in enumerate(scaled(parts)):
             normed[c, rows, :] = part
         return carry
@@ -536,9 +555,13 @@
     return pl.pallas_call(
         functools.partial(kernel, n_ep, topk, cap),
         out_shape=jax.ShapeDtypeStruct((n_rows, width), BF16),
-        in_specs=[vmem] * 4 + [hbm] * 6,
+        in_specs=[hbm] * 10,
         out_specs=vmem,
         scratch_shapes=[
+            tall(n_rows),
+            pltpu.VMEM((1, width), F32),
+            pltpu.VMEM((topk, n_rows), jnp.int32),
+            pltpu.VMEM((topk, n_rows), F32),
             tall(n_rows),
             pltpu.VMEM((2, 8, n_rows), F32),
             pltpu.VMEM((2, 2, 2, 8, n_rows), F32),
@@ -557,6 +580,7 @@
             pltpu.VMEM((2,) + w.shape, BF16)
             for w in (w_gate, w_up, w_down, s_gate, s_up, s_down)
         ]
+        + [dma((3,)), dma((chunks,))]
         + [dma((6,))] * 3
         + [dma((1,)), dma((2, 2, 2))]
         + [dma((chunks,)), per_side] * 2
@@ -564,9 +588,9 @@
         + [per_side]
         + [dma((chunks,)), per_side] * 2,
         compiler_params=pltpu.CompilerParams(
-            collective_id=0, has_side_effects=True, vmem_limit_bytes=VMEM_MIB * 1024 * 1024
+            collective_id=0, has_side_effects=True, vmem_limit_bytes=52 * 1024 * 1024
         ),
-    )(
+    )(*[pltpu.with_memory_space_constraint(a, pltpu.HBM) for a in (
         tokens,
         norm_gain.reshape(1, width),
         expert_ids.T,
@@ -577,7 +601,7 @@
         s_gate,
         s_up,
         s_down,
-    )
+    )])
 
 
 def solution(mesh):

time: 185 us -> 181 us (0.978)
  Pallas kernels: 183 us -> 178 us
    pallas_call x1, Pallas kernels: 183 us -> 178 us  [body(): pl.pallas_call(functools.partial(kernel, n_ep, topk, cap), out_shape=jax....]
where the time goes in v5:
time: 181 us; the launch traced here: 179 us
  Pallas kernels  178 us (98%)
    pallas_call x1, Pallas kernels, body(): pl.pallas_call(functools.partial(kernel, n_ep, topk, cap), out_shape=jax....  178 us

profile of v5, /device:TPU:513, one launch (start us, length us, event | category | flops | bytes accessed | tf_op | source)
XLA Modules:
  0.0 179.2 jit_solution(11952134486651446363)
XLA Ops:
  0.0 178.2 %shard_map.100 = bf16[256,2048]{1,0:T(8,128)(2,1)S(1)} custom-call(bf16[256,2048]{1,0:T(8,128)(2,1)} %tokens_in.1, f32[1,2048]{1,0:T(1,128)} %bitcast.3, s32[2,256]{1,0:T(2,128)} %bitcast.4, f32[2,256]{1,0:T(2,128)} %bitcast.5, bf16[2,2048,256]{2,1,0:T(8,128)(2,1)} %w_gate.1, bf16[2,2048,256]{2,1,0:T(8,128)(2,1)} %w_up.1, bf16[2,256,2048]{2,1,0:T(8,128)(2,1)} %w_down.1, ...), custom_call_target="tpu_custom_call" | custom-call | tf_op jit(solution)/shard_map/pallas_call | solution.py:555
  178.2 1.0 copy.12

commit v6 on v5

--- a/solution.py
+++ b/solution.py
@@ -10,7 +10,6 @@
 
 MESH = pl.DeviceIdType.MESH
 BF16, F32 = jnp.bfloat16, jnp.float32
-VMEM_MIB = 62
 
 
 def silu_mul(first, second):
@@ -434,6 +433,39 @@
                 home_recv,
             )
 
+    far_rows, own_count = reach * local_exp * line, local_exp * line
+    for c in range(chunks):
+        wait_for(dense.at[c], dense_send.at[c])
+
+    def own_row(axis):
+        i = lax.broadcasted_iota(jnp.int32, (1, own_count), 1)
+        return (i // line * side + at[axis]) * line + lax.rem(i, line)
+
+    for axis in range(2):
+        for s in range(2):
+            i = lax.broadcasted_iota(jnp.int32, (1, far_rows), 1)
+            d = i // own_count
+            j_row = lax.rem(i // line, local_exp)
+            pos = lax.rem(at[axis] + (d if s == 0 else side - d), side)
+            row = (j_row * side + pos) * line + lax.rem(i, line)
+            mine = span(side // 2, s)
+            second = lax.rem(i, line) // cap
+            inside = (second >= mine.start) & (second < mine.start + mine.size)
+            row = jnp.where((d < reach - 1) | inside, row, -1)
+            high, low = weigh_rows(notes_in[axis, s, 1], row)
+            normed[2 * axis + s, :, :far_rows] = high
+            tokens[2 * axis + s, :, :far_rows] = low
+            high, low = weigh_rows(notes_in[axis, s, 0], own_row(axis))
+            normed[2 * axis + s, :, far_rows : far_rows + own_count] = high
+            tokens[2 * axis + s, :, far_rows : far_rows + own_count] = low
+
+    def product(weights, rows):
+        rows = jnp.concatenate(rows, axis=0)
+        return sum(jnp.dot(w, rows, preferred_element_type=F32) for w in weights)
+
+    def own_rows(c, pos):
+        return [passing_back[c, j, pos].reshape(line, cols) for j in range(local_exp)]
+
     for j in range(local_exp):
         for c in range(chunks):
             axis = first_axis(c)
@@ -450,68 +482,49 @@
                         hub_recv.at[c, s],
                     )
 
-    def weigh_own(notes, axis):
-        i = lax.broadcasted_iota(jnp.int32, (1, local_exp * line), 1)
-        row = (i // line * side + at[axis]) * line + lax.rem(i, line)
-        return weigh_rows(notes, row)
-
-    def own_rows(c, pos):
-        return [passing_back[c, j, pos].reshape(line, cols) for j in range(local_exp)]
-
-    def product(weights, rows):
-        rows = jnp.concatenate(rows, axis=0)
-        return sum(jnp.dot(w, rows, preferred_element_type=F32) for w in weights)
-
     for axis in range(2):
-        weights = weigh_own(notes_out[axis], axis)
+        weights = weigh_rows(notes_out[axis], own_row(axis))
         for c in range(axis, chunks, 2):
             total[c] += product(weights, own_rows(c, at[axis]))
 
-    for c in range(chunks):
+    both_axes = [(c + axis, s) for c in range(0, chunks, 2) for s in range(2) for axis in range(2)]
+
+    for c, s in both_axes:
         axis = first_axis(c)
-        wait_for(dense.at[c], far_send.at[c])
-        for s in range(2):
-            i = lax.broadcasted_iota(jnp.int32, (1, reach * local_exp * line), 1)
-            d = i // (local_exp * line)
-            j_row = lax.rem(i // line, local_exp)
-            pos = lax.rem(at[axis] + (d if s == 0 else side - d), side)
-            row = (j_row * side + pos) * line + lax.rem(i, line)
-            mine = span(side // 2, s)
-            second = lax.rem(i, line) // cap
-            inside = (second >= mine.start) & (second < mine.start + mine.size)
-            row = jnp.where((d < reach - 1) | inside, row, -1)
-            weights = weigh_rows(notes_in[axis, s, 1], row)
-            rows = own_rows(c, ahead(axis, 1 - s, 2))
-            if reach > 1:
-                wait_for(
-                    arrived.at[c, 0, pl.ds(0, relayed * local_exp // 2)], hub_recv.at[c, s]
-                )
-                rows += [packed_back[c, s].reshape((reach - 1) * local_exp * line, cols)]
-            dense_far[c, s] = product(weights, rows).astype(BF16)
-            to_peer(
-                axis,
-                ahead(axis, 1 - s, 1),
-                dense_far.at[c, s],
-                chain.at[c, s],
-                chain_send.at[c],
-                chain_recv.at[c, s],
-            )
-
-    for c in range(chunks):
+        if s == 0:
+            wait_for(dense.at[c], far_send.at[c])
+        rows = own_rows(c, ahead(axis, 1 - s, 2))
+        if reach > 1:
+            wait_for(arrived.at[c, 0, pl.ds(0, relayed * local_exp // 2)], hub_recv.at[c, s])
+            rows += [packed_back[c, s].reshape((reach - 1) * own_count, cols)]
+        at_gates = 2 * axis + s
+        weights = normed[at_gates, :, :far_rows], tokens[at_gates, :, :far_rows]
+        dense_far[c, s] = product(weights, rows).astype(BF16)
+        to_peer(
+            axis,
+            ahead(axis, 1 - s, 1),
+            dense_far.at[c, s],
+            chain.at[c, s],
+            chain_send.at[c],
+            chain_recv.at[c, s],
+        )
+
+    for c, s in both_axes:
         axis = first_axis(c)
-        for s in range(2):
-            source = ahead(axis, 1 - s, 1)
-            part = product(weigh_own(notes_in[axis, s, 0], axis), own_rows(c, source))
-            wait_for(chain.at[c, s], chain_recv.at[c, s])
-            dense[c, s] = (part + chain[c, s].astype(F32)).astype(BF16)
-            to_peer(
-                axis,
-                source,
-                dense.at[c, s],
-                dense_back.at[c, 1 - s],
-                sum_send.at[c],
-                sum_recv.at[c, 1 - s],
-            )
+        source = ahead(axis, 1 - s, 1)
+        own = slice(far_rows, far_rows + own_count)
+        weights = normed[2 * axis + s, :, own], tokens[2 * axis + s, :, own]
+        part = product(weights, own_rows(c, source))
+        wait_for(chain.at[c, s], chain_recv.at[c, s])
+        dense[c, s] = (part + chain[c, s].astype(F32)).astype(BF16)
+        to_peer(
+            axis,
+            source,
+            dense.at[c, s],
+            dense_back.at[c, 1 - s],
+            sum_send.at[c],
+            sum_recv.at[c, 1 - s],
+        )
 
     for c in range(chunks):
         for s in range(2):
@@ -523,7 +536,6 @@
         copy.wait_send()
     wait_for(notes_in, note_send.at[0])
     for c in range(chunks):
-        wait_for(dense.at[c], dense_send.at[c])
         wait_for(dense.at[c], chain_send.at[c])
         wait_for(dense.at[c], sum_send.at[c])
         for j in range(local_exp):

time: 181 us -> 181 us (level)
  no operation moved by 1% of the time
where the time goes in v6:
time: 181 us; the launch traced here: 179 us
  Pallas kernels  178 us (98%)
    pallas_call x1, Pallas kernels, body(): pl.pallas_call(functools.partial(kernel, n_ep, topk, cap), out_shape=jax....  178 us

profile of v6, /device:TPU:513, one launch (start us, length us, event | category | flops | bytes accessed | tf_op | source)
XLA Modules:
  0.0 179.2 jit_solution(14798147256910158574)
XLA Ops:
  0.0 178.2 %shard_map.100 = bf16[256,2048]{1,0:T(8,128)(2,1)S(1)} custom-call(bf16[256,2048]{1,0:T(8,128)(2,1)} %tokens_in.1, f32[1,2048]{1,0:T(1,128)} %bitcast.3, s32[2,256]{1,0:T(2,128)} %bitcast.4, f32[2,256]{1,0:T(2,128)} %bitcast.5, bf16[2,2048,256]{2,1,0:T(8,128)(2,1)} %w_gate.1, bf16[2,2048,256]{2,1,0:T(8,128)(2,1)} %w_up.1, bf16[2,256,2048]{2,1,0:T(8,128)(2,1)} %w_down.1, ...), custom_call_target="tpu_custom_call" | custom-call | tf_op jit(solution)/shard_map/pallas_call | solution.py:567
  178.2 1.0 copy.12

commit v7 on v5

--- a/solution.py
+++ b/solution.py
@@ -108,14 +108,11 @@
 
     barrier = pltpu.get_barrier_semaphore()
     pl.semaphore_signal(barrier, inc=1, device_id={"tp": 1 - tp}, device_id_type=MESH)
-    for axis in range(2):
-
-        def greet(i, carry):
-            to = peer(axis, lax.rem(at[axis] + i, side))
+    near = sorted({1, 2, side - 1, side - 2})
+    for step in near:
+        for axis in range(2):
+            to = peer(axis, lax.rem(at[axis] + step, side))
             pl.semaphore_signal(barrier, inc=1, device_id={"ep": to}, device_id_type=MESH)
-            return carry
-
-        lax.fori_loop(1, side, greet, 0)
 
     pairs = ((s_gate, sg), (s_up, su), (s_down, sd), (w_gate, wg), (w_up, wu), (w_down, wd))
     local = [
@@ -146,7 +143,7 @@
     for copy in token_loads[:2] + small_loads + token_loads[2:] + local:
         copy.start()
 
-    pl.semaphore_wait(barrier, 2 * side - 1)
+    pl.semaphore_wait(barrier, 2 * len(near) + 1)
 
     def to_peer(axis, pos, src, dst, send_sem, recv_sem):
         pltpu.make_async_remote_copy(
@@ -376,8 +373,10 @@
 
     for j in range(local_exp):
         for c in range(chunks):
-            if relayed:
-                wait_for(arrived.at[c, 0, pl.ds(0, relayed)], relay_recv.at[c, j])
+            first = j == 0 and c < 2
+            for d in ((0, 1) if first and c == 0 else () if first else (c,)):
+                if relayed:
+                    wait_for(arrived.at[d, 0, pl.ds(0, relayed)], relay_recv.at[d, j])
             across(
                 j,
                 c,

time: 181 us -> 181 us (level)
  no operation moved by 1% of the time
where the time goes in v7:
time: 181 us; the launch traced here: 179 us
  Pallas kernels  178 us (98%)
    pallas_call x1, Pallas kernels, body(): pl.pallas_call(functools.partial(kernel, n_ep, topk, cap), out_shape=jax....  178 us

profile of v7, /device:TPU:513, one launch (start us, length us, event | category | flops | bytes accessed | tf_op | source)
XLA Modules:
  0.0 179.2 jit_solution(1787465951524037222)
XLA Ops:
  0.0 178.2 %shard_map.100 = bf16[256,2048]{1,0:T(8,128)(2,1)S(1)} custom-call(bf16[256,2048]{1,0:T(8,128)(2,1)} %tokens_in.1, f32[1,2048]{1,0:T(1,128)} %bitcast.3, s32[2,256]{1,0:T(2,128)} %bitcast.4, f32[2,256]{1,0:T(2,128)} %bitcast.5, bf16[2,2048,256]{2,1,0:T(8,128)(2,1)} %w_gate.1, bf16[2,2048,256]{2,1,0:T(8,128)(2,1)} %w_up.1, bf16[2,256,2048]{2,1,0:T(8,128)(2,1)} %w_down.1, ...), custom_call_target="tpu_custom_call" | custom-call | tf_op jit(solution)/shard_map/pallas_call | solution.py:554
  178.2 1.0 copy.12
